TPU v7x, 32 devices: a whole 2x2x4 slice. The times are simulated.
32 devices in a mesh: sp: 8 (over z, y), tp: 4 (over x, core).
Axes of the slice: x: 2, y: 2, z: 4, core: 2. Of those that a mesh axis runs over, the one named last changes fastest.
Arguments:
- d_out: bfloat16 [4096, 2048], P('sp'), may hold values from -6 to 6
- route_expert: int32 [4096, 2], P('sp'), may hold values from 0 to 7, all different within a row; in each aligned block of 512 rows (0 to 511, 512 to 1023, ...) at most 144 rows name the same one
- route_weight: float32 [4096, 2], P('sp'), may hold values from 0.2 to 1
- expert_inputs: bfloat16 [8, 1152, 2048], P('sp'), may hold values from -6 to 6
- w_gate: bfloat16 [8, 2048, 2816], P('sp', None, 'tp'), may hold values from -0.125 to 0.125
- w_up: bfloat16 [8, 2048, 2816], P('sp', None, 'tp'), may hold values from -0.125 to 0.125
- w_down: bfloat16 [8, 2816, 2048], P('sp', 'tp'), may hold values from -0.109375 to 0.109375
- w_out: bfloat16 [2048, 1024], P(None, 'tp'), may hold values from -0.1875 to 0.1875
- queries: bfloat16 [4096, 4, 128], P('sp', 'tp'), may hold values from -6 to 6
- keys: bfloat16 [4096, 4, 128], P('sp', 'tp'), may hold values from -2 to 2
- values: bfloat16 [4096, 4, 256], P('sp', 'tp'), may hold values from -6 to 6
- log_decay: float32 [4096, 4, 128], P('sp', 'tp'), may hold values from -1 to 0
Outputs:
- grad_gate: bfloat16 [8, 2048, 2816], P('sp', None, 'tp')
- grad_up: bfloat16 [8, 2048, 2816], P('sp', None, 'tp')
- grad_down: bfloat16 [8, 2816, 2048], P('sp', 'tp')
- grad_proj: float32 [2048, 1024], P('sp', 'tp')
- grad_queries: bfloat16 [4096, 4, 128], P('sp', 'tp')
- grad_keys: bfloat16 [4096, 4, 128], P('sp', 'tp')
- grad_values: bfloat16 [4096, 4, 256], P('sp', 'tp')
- grad_log_decay: float32 [4096, 4, 128], P('sp', 'tp')
Inputs may be any that keep to these rules, and one draw needn't show every extreme that they name: `route_expert`: the two experts of a token differ. Among the rows of one device no expert is named more than 144 times, and in every draw some device names some expert exactly 144 times.
All inputs are finite; a program needn't handle non-finite values.
Results may differ from a plain program's by a relative error of at most 0.02.
Values may be sent and summed in bfloat16 or wider, within the bound.
A program may use at most 128 MiB of HBM per device.

v0:
```python
import jax
import jax.numpy as jnp
from jax import lax
from jax.sharding import PartitionSpec as P

BLK = 64


precise = lax.Precision.HIGHEST


def carried_in(x, axis, combine, identity, reverse):
    count, index = (lax.axis_size(axis), lax.axis_index(axis))
    everything = jax.tree.map(
        lambda part, kind: lax.all_gather(part.astype(kind), axis), x, (jnp.bfloat16, jnp.bfloat16)
    )
    start = jax.tree.map(
        lambda part, zero: jnp.broadcast_to(jnp.asarray(zero, part.dtype), part.shape), x, identity
    )

    def step(k, before):
        at = count - 1 - k if reverse else k
        reached = at > index if reverse else at < index
        new = combine(
            before, jax.tree.map(lambda part, own: part[at].astype(own.dtype), everything, x)
        )
        return jax.tree.map(lambda a, b: jnp.where(reached, a, b), new, before)

    return lax.fori_loop(0, count, step, start)


def block_mixer(scaled_queries, keys_in, values_in, decay_in, initial):
    length, head_count, _ = scaled_queries.shape
    value_width = values_in.shape[-1]
    count_blocks = length // BLK

    def to_blocks(tensor):
        return tensor.reshape(count_blocks, BLK, head_count, tensor.shape[-1]).transpose(0, 2, 1, 3)

    causal = jnp.tril(jnp.ones((BLK, BLK), dtype=bool))[:, :, None]

    def advance(carry_state, inputs):
        query_block, key_block, value_block, decay_block = inputs
        cumulative = jnp.cumsum(decay_block, axis=1)
        ending = cumulative[:, -1, :]
        carried = jnp.einsum(
            "hcd,hde->hce", query_block * jnp.exp(cumulative), carry_state, precision=precise
        )
        within = jnp.where(
            causal, jnp.exp(cumulative[:, :, None, :] - cumulative[:, None, :, :]), 0.0
        )
        scores = jnp.einsum("hid,hjd,hijd->hij", query_block, key_block, within, precision=precise)
        inner_part = jnp.einsum("hij,hje->hie", scores, value_block, precision=precise)
        faded_keys = key_block * jnp.exp(ending[:, None, :] - cumulative)
        carry_state = carry_state * jnp.exp(ending)[:, :, None] + jnp.einsum(
            "hcd,hce->hde", faded_keys, value_block, precision=precise
        )
        return (carry_state, carried + inner_part)

    final_state, blocks_out = lax.scan(
        jax.checkpoint(advance),
        initial,
        (to_blocks(scaled_queries), to_blocks(keys_in), to_blocks(values_in), to_blocks(decay_in)),
    )
    return (blocks_out.transpose(0, 2, 1, 3).reshape(length, head_count, value_width), final_state)


def expert_pass(rows_in, routed_rows, gate_w, up_w, down_w):
    gate_pre = jnp.dot(rows_in, gate_w, preferred_element_type=jnp.float32)
    up_pre = jnp.dot(rows_in, up_w, preferred_element_type=jnp.float32)
    sigmoid_gate = jax.nn.sigmoid(gate_pre)
    active = gate_pre * sigmoid_gate
    hidden = (active * up_pre).astype(jnp.bfloat16)
    d_hidden = lax.dot_general(
        routed_rows, down_w, (((1,), (1,)), ((), ())), preferred_element_type=jnp.float32
    )
    d_gate = (d_hidden * up_pre * sigmoid_gate * (1.0 + gate_pre * (1.0 - sigmoid_gate))).astype(
        jnp.bfloat16
    )
    d_up = (d_hidden * active).astype(jnp.bfloat16)
    rows_first = (((0,), (0,)), ((), ()))
    grad_gate = lax.dot_general(
        rows_in, d_gate, rows_first, preferred_element_type=jnp.float32
    ).astype(jnp.bfloat16)
    grad_up = lax.dot_general(rows_in, d_up, rows_first, preferred_element_type=jnp.float32).astype(
        jnp.bfloat16
    )
    grad_down = lax.dot_general(
        hidden, routed_rows, rows_first, preferred_element_type=jnp.float32
    ).astype(jnp.bfloat16)
    return (grad_gate, grad_up, grad_down, d_gate, d_up)


def chain(earlier, later):
    return (earlier[0] * later[0], later[0][..., None] * earlier[1] + later[1])


def local(
    d_out,
    route_expert,
    route_weight,
    expert_inputs,
    w_gate,
    w_up,
    w_down,
    w_out,
    queries,
    keys,
    values,
    log_decay,
):
    tok_rows = d_out.shape[0]
    model_width = d_out.shape[1]
    experts = lax.axis_size("sp")
    capacity = expert_inputs.shape[1] // experts
    flat_experts = route_expert.reshape(-1)
    onehot = (flat_experts[:, None] == jnp.arange(experts, dtype=jnp.int32)[None, :]).astype(
        jnp.int32
    )
    before = jnp.cumsum(onehot, axis=0) - onehot
    rank_slot = jnp.sum(before * onehot, axis=1)
    slot_index = flat_experts * capacity + rank_slot
    quarter = model_width // lax.axis_size("tp")
    column_start = lax.axis_index("tp") * quarter
    own_cols = lax.dynamic_slice_in_dim(d_out, column_start, quarter, 1)
    scaled = (
        jnp.repeat(own_cols, 2, axis=0).astype(jnp.float32) * route_weight.reshape(-1)[:, None]
    ).astype(jnp.bfloat16)
    outbox = (
        jnp.zeros((experts * capacity, own_cols.shape[1]), jnp.bfloat16).at[slot_index].set(scaled)
    )
    outbox = outbox.reshape(experts, capacity, own_cols.shape[1])
    partial_rows = lax.all_to_all(outbox, "sp", split_axis=0, concat_axis=0, tiled=True)
    routed = lax.all_gather(partial_rows, "tp", axis=2, tiled=True)
    routed = routed.reshape(experts * capacity, model_width)
    rows_in = expert_inputs[0]
    gate_w = w_gate[0]
    up_w = w_up[0]
    grad_gate, grad_up, grad_down, d_gate, d_up = expert_pass(
        rows_in, routed, gate_w, up_w, w_down[0]
    )
    partial_terms = lax.dot_general(
        d_gate, gate_w, (((1,), (1,)), ((), ())), preferred_element_type=jnp.float32
    )
    partial_terms = partial_terms + lax.dot_general(
        d_up, up_w, (((1,), (1,)), ((), ())), preferred_element_type=jnp.float32
    )
    rounded = lax.optimization_barrier(partial_terms.astype(jnp.bfloat16)).astype(jnp.float32)
    summed = lax.psum_scatter(rounded.astype(jnp.bfloat16), "tp", scatter_dimension=1, tiled=True)
    returned = lax.all_to_all(
        summed.reshape(experts, capacity, quarter), "sp", split_axis=0, concat_axis=0, tiled=True
    )
    picked = returned.reshape(experts * capacity, quarter)[slot_index].astype(jnp.float32)
    picked = picked.reshape(tok_rows, 2, quarter).sum(axis=1)
    mix_cols = (own_cols.astype(jnp.float32) + picked).astype(jnp.bfloat16)
    mix_grad = lax.all_gather(mix_cols, "tp", axis=1, tiled=True)
    scale_q = queries.shape[2] ** (-0.5)
    query_f = queries.astype(jnp.float32)
    key_f = keys.astype(jnp.float32)
    value_f = values.astype(jnp.float32)
    cumulative = jnp.cumsum(log_decay, axis=0)
    ending = cumulative[-1]
    carry_decay = jnp.exp(ending)
    produced = jnp.einsum(
        "thd,the->hde", key_f * jnp.exp(ending[None] - cumulative), value_f, precision=precise
    )
    identity = (jnp.ones_like(carry_decay), jnp.zeros_like(produced))
    start_state = carried_in((carry_decay, produced), "sp", chain, identity, False)[1]

    def local_map(query_x, key_x, value_x, decay_x):
        return block_mixer(query_x * scale_q, key_x, value_x, decay_x, start_state)

    (mixer_out, _), pullback = jax.vjp(local_map, query_f, key_f, value_f, log_decay)
    head_local = mixer_out.shape[1]
    value_width = mixer_out.shape[2]
    mixed = mixer_out.reshape(tok_rows, head_local * value_width).astype(jnp.bfloat16)
    grad_proj = lax.psum_scatter(
        lax.dot_general(
            mix_grad, mixed, (((0,), (0,)), ((), ())), preferred_element_type=jnp.float32
        ).astype(jnp.bfloat16),
        "sp",
        scatter_dimension=0,
        tiled=True,
    ).astype(jnp.float32)
    d_mixed = jnp.dot(mix_grad, w_out, preferred_element_type=jnp.float32).reshape(
        tok_rows, head_local, value_width
    )
    own_term = jnp.einsum(
        "thd,the->hde", query_f * scale_q * jnp.exp(cumulative), d_mixed, precision=precise
    )
    later_grad = carried_in((carry_decay, own_term), "sp", chain, identity, True)[1]
    grad_q, grad_k, grad_v, grad_g = pullback((d_mixed, later_grad))
    return (
        grad_gate[None],
        grad_up[None],
        grad_down[None],
        grad_proj,
        grad_q.astype(jnp.bfloat16),
        grad_k.astype(jnp.bfloat16),
        grad_v.astype(jnp.bfloat16),
        grad_g,
    )


def solution(mesh):
    return jax.shard_map(
        local,
        mesh=mesh,
        in_specs=(
            P("sp", None),
            P("sp", None),
            P("sp", None),
            P("sp", None, None),
            P("sp", None, "tp"),
            P("sp", None, "tp"),
            P("sp", "tp", None),
            P(None, "tp"),
            P("sp", "tp", None),
            P("sp", "tp", None),
            P("sp", "tp", None),
            P("sp", "tp", None),
        ),
        out_specs=(
            P("sp", None, "tp"),
            P("sp", None, "tp"),
            P("sp", "tp", None),
            P("sp", "tp"),
            P("sp", "tp", None),
            P("sp", "tp", None),
            P("sp", "tp", None),
            P("sp", "tp", None),
        ),
        check_vma=False,
    )
```

profile of v0, /device:TPU:0, one launch (start us, length us, event | category | flops | bytes accessed | tf_op | source)
XLA Modules:
  0.0 436.2 jit_solution(9590582344424962027)
XLA Ops:
  15.6 3.7 convert_element_type.210
  19.6 7.2 %scatter_custom_fusion = bf16[1152,512]{1,0:T(8,128)(2,1)} fusion(s32[1024]{0:T(1024)S(1)} %bitcast.512, f32[1024,512]{1,0:T(8,128)} %convert_element_type.210, f32[1024]{0:T(1024)S(1)} %mul.286, bf16[]{:T(256)} %constant.180.clone.1), kind=kCustom, calls=%fused_computation.141 | custom fusion | flops 1048576 | bytes 3280898 | tf_op jit(solution)/shard_map/scatter | solution.py:130
  26.9 36.3 %all_to_all.10 = bf16[8,144,512]{2,1,0:T(8,128)(2,1)} all-to-all(bf16[8,144,512]{2,1,0:T(8,128)(2,1)} %bitcast.498), channel_id=1, replica_groups=mesh['sp'=8,'tp'=4] {'sp'}, dimensions={0} | all-to-all | bytes 2359296 | tf_op jit(solution)/shard_map/all_to_all | solution.py:133
  63.5 8.2 %fusion.74 = f32[1152,704]{0,1:T(8,128)} fusion(bf16[1,1152,2048]{2,1,0:T(8,128)(2,1)} %param.23, bf16[1,2048,704]{1,2,0:T(8,128)(2,1)S(1)} %copy-done), kind=kOutput, calls=%fused_computation.115 | convolution fusion | flops 3321888768 | bytes 10846208 | tf_op jit(solution)/shard_map/dot_general | solution.py:69
  71.6 8.1 %fusion.76 = f32[1152,704]{0,1:T(8,128)} fusion(bf16[1,1152,2048]{2,1,0:T(8,128)(2,1)} %param.23, bf16[1,2048,704]{1,2,0:T(8,128)(2,1)S(1)} %copy-done.7), kind=kOutput, calls=%fused_computation.117 | convolution fusion | flops 3321888768 | bytes 10846208 | tf_op jit(solution)/shard_map/dot_general | solution.py:70
  79.7 19.7 %all-gather.5.cloned.1.call-done = bf16[8,144,2048]{2,1,0:T(8,128)(2,1)} async-done(((bf16[8,144,512]{2,1,0:T(8,128)(2,1)}), bf16[8,144,2048]{2,1,0:T(8,128)(2,1)}) %all-gather.5.cloned.1.call-update) | async-done | bytes 4718608 | tf_op jit(solution)/shard_map/all_gather | solution.py:134
  99.5 9.7 %multiply_convert_fusion.1 = (bf16[1152,704]{0,1:T(8,128)(2,1)S(1)}, bf16[1152,704]{0,1:T(8,128)(2,1)S(1)}) fusion(f32[1152,704]{0,1:T(8,128)} %fusion.74, f32[1152,704]{0,1:T(8,128)} %fusion.76, bf16[1152,2048]{1,0:T(8,128)(2,1)} %bitcast.515, bf16[1,704,2048]{2,1,0:T(8,128)(2,1)} %param.26), kind=kOutput, calls=%fused_computation.123 | convolution fusion | flops 3332431872 | bytes 17334272 | tf_op jit(solution)/shard_map/dot_general | solution.py:74
  109.2 4.1 fusion.92
  113.4 5.6 %add_convert_fusion = bf16[1152,2048]{1,0:T(8,128)(2,1)} fusion(f32[1152,2048]{1,0:T(8,128)S(1)} %fusion.92, bf16[1152,704]{0,1:T(8,128)(2,1)S(1)} %get-tuple-element.877, bf16[1,2048,704]{1,2,0:T(8,128)(2,1)S(1)} %copy-done.8), kind=kOutput, calls=%fused_computation.110 | convolution fusion | flops 3326607360 | bytes 18661376 | tf_op jit(solution)/shard_map/dot_general | solution.py:145
  120.5 20.5 %all_gather.26 = bf16[8,1,128]{2,1,0:T(2,128)(2,1)S(1)} all-gather(bf16[1,1,128]{2,1,0:T(2,128)(2,1)S(1)} %get-tuple-element.880), channel_id=1, replica_groups=mesh['sp'=8,'tp'=4] {'sp'}, dimensions={0}, use_global_device_ids=true | all-gather | bytes 2304 | tf_op jit(solution)/shard_map/all_gather | solution.py:15
  141.4 31.4 %all-gather = bf16[1024,256]{1,0:T(8,128)(2,1)S(1)} all-gather(bf16[128,256]{1,0:T(8,128)(2,1)S(1)} %convolution_convert_fusion.3), channel_id=2, replica_groups=mesh['sp'=8,'tp'=4] {'sp'}, dimensions={0}, use_global_device_ids=true | all-gather | bytes 589824 | tf_op jit(solution)/shard_map/all_gather | solution.py:15
  173.6 3.6 all-to-all-start.1
  178.3 22.9 %all-to-all-done.1 = bf16[8,144,512]{2,1,0:T(8,128)(2,1)S(1)} async-done(((bf16[8,144,512]{2,1,0:T(8,128)(2,1)}), bf16[8,144,512]{2,1,0:T(8,128)(2,1)S(1)}, u32[]{:S(2)}, u32[]{:S(2)}) %all-to-all-start.1) | async-done | bytes 1179680 | tf_op jit(solution)/shard_map/all_to_all | solution.py:150
  201.2 5.1 %gather_fusion = bf16[1024,512]{1,0:T(8,128)(2,1)} fusion(bf16[1152,512]{1,0:T(8,128)(2,1)S(1)} %bitcast.487, s32[1024]{0:T(1024)S(1)} %broadcast_clamp_fusion), kind=kCustom, calls=%fused_computation | custom fusion | bytes 2101248 | tf_op jit(solution)/shard_map/gather | solution.py:153
  206.3 2.4 reshape.829
  208.7 3.7 reduce_sum.58
  212.4 2.3 add_convert_fusion.1
  215.8 54.8 %while.69 = (s32[]{:T(128)}, f32[1,128,256]{2,1,0:T(8,128)S(1)}, bf16[8,1,64,256]{3,2,1,0:T(8,128)(2,1)}, f32[8,1,128,256]{3,2,1,0:T(8,128)}, f32[8,1,64,128]{3,...) while((s32[]{:T(128)}, f32[1,128,256]{2,1,0:T(8,128)S(1)}, ...), condition=%wide.region_12.13_spmd.clone, body=%wide.region_10.12_spmd.clone.sunk | while | flops 66154496 | bytes 5727369 | solution.py:60
  271.2 8.4 %fusion.89 = bf16[1,2048,704]{1,2,0:T(8,128)(2,1)} fusion(bf16[1152,704]{0,1:T(8,128)(2,1)} %copy-done.10, bf16[1,1152,2048]{2,1,0:T(8,128)(2,1)} %param.23), kind=kOutput, calls=%fused_computation.129 | convolution fusion | flops 3323330560 | bytes 9224192 | tf_op jit(solution)/shard_map/dot_general | solution.py:82
  279.7 7.7 %fusion.86 = bf16[1,2048,704]{1,2,0:T(8,128)(2,1)} fusion(bf16[1152,704]{0,1:T(8,128)(2,1)S(1)} %copy-done.14, bf16[1,1152,2048]{2,1,0:T(8,128)(2,1)} %param.23), kind=kOutput, calls=%fused_computation.128 | convolution fusion | flops 3323330560 | bytes 9224192 | tf_op jit(solution)/shard_map/dot_general | solution.py:85
  287.4 5.4 %fusion.85 = bf16[1,704,2048]{2,1,0:T(8,128)(2,1)} fusion(bf16[1152,2048]{1,0:T(8,128)(2,1)S(1)} %bitcast.518, f32[1152,704]{0,1:T(8,128)S(1)} %copy-done.12, f32[1152,704]{0,1:T(8,128)S(1)} %copy-done.11), kind=kOutput, calls=%fused_computation.127 | convolution fusion | flops 3328196608 | bytes 14090240 | tf_op jit(solution)/shard_map/dot_general | solution.py:88
  292.8 3.4 convolution_convert_fusion.1
  299.2 32.5 %all-gather.1 = bf16[1024,256]{1,0:T(8,128)(2,1)S(1)} all-gather(bf16[128,256]{1,0:T(8,128)(2,1)S(1)} %convolution_convert_fusion.2), channel_id=3, replica_groups=mesh['sp'=8,'tp'=4] {'sp'}, dimensions={0}, use_global_device_ids=true | all-gather | bytes 589824 | tf_op jit(solution)/shard_map/all_gather | solution.py:15
  334.4 92.2 %while.70 = (s32[]{:T(128)}, f32[1,128,256]{1,2,0:T(8,128)S(1)}, f32[8,1,64,128]{3,2,1,0:T(8,128)S(1)}, bf16[8,1,64,128]{3,2,1,0:T(8,128)(2,1)}, bf16[8,1,64,256...) while((s32[]{:T(128)}, f32[1,128,256]{1,2,0:T(8,128)S(1)}, ...), condition=%wide.region_23.24_spmd.clone, body=%wide.region_16.23_spmd.clone.sunk | while | flops 137650176 | bytes 3924165 | solution.py:60
  (404 shorter events, 170.2 us)
Async XLA Ops:
  7.2 56.3 %copy-start = (bf16[1,2048,704]{1,2,0:T(8,128)(2,1)S(1)}, bf16[1,2048,704]{1,2,0:T(8,128)(2,1)}, u32[]{:S(2)}) copy-start(bf16[1,2048,704]{1,2,0:T(8,128)(2,1)} %param.24) | copy-start | bytes 8650756
  7.2 92.3 %all-gather.5.cloned.1.call-start = ((), (), s32[]{:S(2)}) async-start(), calls=%async_computation.4 | async-start | bytes 5898240 | tf_op jit(solution)/shard_map/all_gather | solution.py:134
  15.6 3.7 copy-start.6
  63.2 110.4 %reduce-scatter.3.cloned.1.call-start = ((), (), s32[]{:S(2)}) async-start(), calls=%async_computation.5 | async-start | bytes 5898240 | tf_op jit(solution)/shard_map/reduce_scatter | solution.py:149
  63.4 8.2 %copy-start.7 = (bf16[1,2048,704]{1,2,0:T(8,128)(2,1)S(1)}, bf16[1,2048,704]{1,2,0:T(8,128)(2,1)}, u32[]{:S(2)}) copy-start(bf16[1,2048,704]{1,2,0:T(8,128)(2,1)} %param.25) | copy-start | bytes 8650756
  109.2 4.2 copy-start.10
  109.2 4.2 copy-start.13
  109.2 4.2 copy-start.8
  119.0 1.3 copy-start.3
  119.0 1.3 copy-start.2
  120.2 52.6 %copy-start.4 = (bf16[512,1,128]{2,0,1:T(8,128)(2,1)S(1)}, bf16[512,1,128]{2,0,1:T(8,128)(2,1)}, u32[]{:S(2)}) copy-start(bf16[512,1,128]{2,0,1:T(8,128)(2,1)} %param.28) | copy-start | bytes 393220
  173.6 27.7 %all-to-all-start.1 = ((bf16[8,144,512]{2,1,0:T(8,128)(2,1)}), bf16[8,144,512]{2,1,0:T(8,128)(2,1)S(1)}, u32[]{:S(2)}, u32[]{:S(2)}) async-start(bf16[8,144,512]{2,1,0:T(8,128)(2,1)} %bitcast.502), calls=%async_computation.2 | async-start | bytes 2359296 | tf_op jit(solution)/shard_map/all_to_all | solution.py:150
  177.1 115.7 %all-gather.7.cloned.1.call-start = ((), (), s32[]{:S(2)}) async-start(), calls=%async_computation.6 | async-start | bytes 2621440 | tf_op jit(solution)/shard_map/all_gather | solution.py:156
  214.7 212.5 %reduce-scatter.5.cloned.1.call-start = ((), (), s32[]{:S(2)}) async-start(), calls=%async_computation.7 | async-start | bytes 1179648 | tf_op jit(solution)/shard_map/reduce_scatter | solution.py:177
  271.2 8.4 %copy-start.14 = (bf16[1152,704]{0,1:T(8,128)(2,1)S(1)}, bf16[1152,704]{0,1:T(8,128)(2,1)}, u32[]{:S(2)}) copy-start(bf16[1152,704]{0,1:T(8,128)(2,1)} %copy-done.13) | copy-start | bytes 4866052
  271.2 16.2 %slice-start = ((s8[4718592]{0:T(1024)(128)(4,1)}), s8[4194304]{0:T(1024)(128)(4,1)S(1)}, s32[]{:S(2)}) async-start(s8[4718592]{0:T(1024)(128)(4,1)} %bitcast.516), calls=%async_computation.8 | async-start | bytes 8388608
  279.7 7.7 %slice-start.1 = ((s8[4718592]{0:T(1024)(128)(4,1)}), s8[524288]{0:T(1024)(128)(4,1)S(1)}, s32[]{:S(2)}) async-start(s8[4718592]{0:T(1024)(128)(4,1)} %bitcast.516), calls=%async_computation.9 | async-start | bytes 1048576
  279.7 7.7 %copy-start.11 = (f32[1152,704]{0,1:T(8,128)S(1)}, f32[1152,704]{0,1:T(8,128)}, u32[]{:S(2)}) copy-start(f32[1152,704]{0,1:T(8,128)} %fusion.74) | copy-start | bytes 9732100
  279.7 7.7 %copy-start.12 = (f32[1152,704]{0,1:T(8,128)S(1)}, f32[1152,704]{0,1:T(8,128)}, u32[]{:S(2)}) copy-start(f32[1152,704]{0,1:T(8,128)} %fusion.76) | copy-start | bytes 9732100
  287.4 5.4 %copy-start.5 = (bf16[8,1,64,256]{3,2,1,0:T(8,128)(2,1)S(1)}, bf16[8,1,64,256]{3,2,1,0:T(8,128)(2,1)}, u32[]{:S(2)}) copy-start(bf16[8,1,64,256]{3,2,1,0:T(8,128)(2,1)} %get-tuple-element.581) | copy-start | bytes 786436
  292.8 3.5 copy-start.9
  426.6 2.5 copy-start.1
Sparse Core Ops, SparseCore 0:
  63.3 36.0 all-gather.4
  119.2 47.8 reduce-scatter.2
  214.9 20.3 all-gather.6
  296.4 63.2 reduce-scatter.4
where the time goes:
time: 444 us; the launch traced here: 436 us
  blocking collectives  121 us (27%)
  matrix products  104 us (23%)
  other arithmetic  87.5 us (20%)
  local copies, waits for them, and re-layouts  60.6 us (14%)
  waiting for transfers between devices  42.7 us (10%)
  between operations  14.6 us (3%)
    all_gather x3, blocking collectives, carried_in(): lax.all_gather(part.astype(kind), axis)  84.4 us
    all_to_all x1, blocking collectives, local(): lax.all_to_all(outbox, 'sp', split_axis=0, concat_axis=0, tiled=True)  36.3 us
    dot_general x24, other arithmetic, advance(): jnp.einsum('hid,hjd,hijd->hij', query_block, key_block, within, precision...  36 us
    all_to_all x1, waiting for transfers between devices, local(): lax.all_to_all(summed.reshape(experts, capacity, quarter), 'sp', split_ax...  22.9 us
    all_gather x1, waiting for transfers between devices, local(): routed = lax.all_gather(partial_rows, 'tp', axis=2, tiled=True)  19.7 us
    squeeze x32, local copies, waits for them, and re-layouts, block_mixer(): lax.scan(jax.checkpoint(advance), initial, (to_blocks(scaled_queries), to...  18.4 us
    reduce_sum x8, other arithmetic, advance(): cumulative[:, :, None, :] - cumulative[:, None, :, :]  17 us
    dot_general x24, matrix products, advance(): jnp.einsum('hij,hje->hie', scores, value_block, precision=precise)  15.7 us
  transfers between devices with their start and end apart: 5, of which 2 were waited for; matrix products, arithmetic and copies ran while one was open for 45% of the time, Pallas kernels for 0%

commit v1 on v0

v1 whole, which is shorter than its diff:
```python
import functools

import jax
import jax.numpy as jnp
from jax import lax
from jax.experimental import pallas as pl
from jax.experimental.pallas import tpu as pltpu
from jax.sharding import PartitionSpec as P

BLK = 64


precise = lax.Precision.HIGHEST


MESH = pl.DeviceIdType.MESH
NN = (((1,), (0,)), ((), ()))
NT = (((1,), (1,)), ((), ()))
TN = (((0,), (0,)), ((), ()))


def mm(a, b, dims):
    return lax.dot_general(a, b, dims, preferred_element_type=jnp.float32)


def triangle(lower):
    rows = lax.broadcasted_iota(jnp.int32, (BLK, BLK), 0)
    cols = lax.broadcasted_iota(jnp.int32, (BLK, BLK), 1)
    return rows >= cols if lower else rows <= cols


def block_sums(mask, x):
    return lax.dot_general(
        mask.astype(jnp.float32), x, NN, precision=precise, preferred_element_type=jnp.float32
    )


def decays(g_ref, rows):
    cumulative = block_sums(triangle(True), g_ref[rows, :])
    middle = cumulative[BLK // 2 - 1 : BLK // 2, :]
    ending = cumulative[BLK - 1 : BLK, :]
    return cumulative, middle, ending


def greet(n, me):
    barrier = pltpu.get_barrier_semaphore()
    for k in range(1, n):
        pl.semaphore_signal(
            barrier, inc=1, device_id={"sp": lax.rem(me + k, n)}, device_id_type=MESH
        )
    return barrier


def state_copies(n, me, step, send_ref, recv_ref, send_sem, recv_sem):
    return [
        pltpu.make_async_remote_copy(
            src_ref=send_ref,
            dst_ref=recv_ref.at[k - 1],
            send_sem=send_sem.at[k - 1],
            recv_sem=recv_sem.at[k - 1],
            device_id={"sp": lax.rem(me + step * k + n, n)},
            device_id_type=MESH,
        )
        for k in range(1, n)
    ]


def collect(n, me, step, copies, recv_ref, total, width):
    total[...] = jnp.zeros_like(total)
    for k in range(n - 1, 0, -1):
        copies[k - 1].wait()
        source = me - step * k
        reached = jnp.logical_and(source >= 0, source < n)

        @pl.when(reached)
        def _():
            factor = recv_ref[k - 1, width : width + 1, :].astype(jnp.float32)
            total[...] = total[...] * factor + recv_ref[k - 1, :width, :].astype(jnp.float32)


def forward_kernel(
    n, scale, q_ref, k_ref, v_ref, g_ref, mixed_ref, states_ref, kept, total, send, recv, ssem, rsem
):
    me = lax.axis_index("sp")
    barrier = greet(n, me)
    length, width = v_ref.shape
    blocks = length // BLK
    causal = triangle(True)
    local = jnp.zeros(total.shape, jnp.float32)
    ahead = jnp.zeros((1, q_ref.shape[1]), jnp.float32)
    befores = []
    for b in range(blocks):
        rows = pl.ds(b * BLK, BLK)
        cumulative, _, ending = decays(g_ref, rows)
        kept[b] = local
        befores.append(ahead)
        faded = (k_ref[rows, :].astype(jnp.float32) * jnp.exp(ending - cumulative)).astype(
            jnp.bfloat16
        )
        local = local * jnp.exp(ending) + mm(v_ref[rows, :], faded, TN)
        ahead = ahead + ending
    send[:width, :] = local.astype(jnp.bfloat16)
    send[width:, :] = jnp.broadcast_to(jnp.exp(ahead), (16, ahead.shape[1])).astype(jnp.bfloat16)
    pl.semaphore_wait(barrier, n - 1)
    copies = state_copies(n, me, 1, send, recv, ssem, rsem)
    for copy in copies:
        copy.start()
    inner = []
    scaled = []
    for b in range(blocks):
        rows = pl.ds(b * BLK, BLK)
        cumulative, middle, _ = decays(g_ref, rows)
        query = q_ref[rows, :].astype(jnp.float32) * scale
        key = k_ref[rows, :].astype(jnp.float32)
        lifted_q = (query * jnp.exp(cumulative - middle)).astype(jnp.bfloat16)
        lifted_k = (key * jnp.exp(middle - cumulative)).astype(jnp.bfloat16)
        scores = jnp.where(causal, mm(lifted_q, lifted_k, NT), 0.0).astype(jnp.bfloat16)
        inner.append(mm(scores, v_ref[rows, :], NN))
        scaled.append((query * jnp.exp(cumulative)).astype(jnp.bfloat16))
    collect(n, me, 1, copies, recv, total, width)
    for b in range(blocks):
        rows = pl.ds(b * BLK, BLK)
        state = (kept[b] + total[...] * jnp.exp(befores[b])).astype(jnp.bfloat16)
        states_ref[b] = state
        mixed_ref[rows, :] = (inner[b] + mm(scaled[b], state, NT)).astype(jnp.bfloat16)


def backward_kernel(
    n,
    scale,
    q_ref,
    k_ref,
    v_ref,
    g_ref,
    d_ref,
    states_ref,
    gq_ref,
    gk_ref,
    gv_ref,
    gg_ref,
    kept,
    total,
    send,
    recv,
    ssem,
    rsem,
):
    me = lax.axis_index("sp")
    barrier = greet(n, me)
    length, width = v_ref.shape
    blocks = length // BLK
    causal = triangle(True)
    local = jnp.zeros(total.shape, jnp.float32)
    after = jnp.zeros((1, q_ref.shape[1]), jnp.float32)
    afters = [None] * blocks
    for b in reversed(range(blocks)):
        rows = pl.ds(b * BLK, BLK)
        cumulative, _, ending = decays(g_ref, rows)
        kept[b] = local
        afters[b] = after
        query = q_ref[rows, :].astype(jnp.float32) * scale
        scaled = (query * jnp.exp(cumulative)).astype(jnp.bfloat16)
        local = local * jnp.exp(ending) + mm(d_ref[rows, :], scaled, TN)
        after = after + ending
    send[:width, :] = local.astype(jnp.bfloat16)
    send[width:, :] = jnp.broadcast_to(jnp.exp(after), (16, after.shape[1])).astype(jnp.bfloat16)
    pl.semaphore_wait(barrier, n - 1)
    copies = state_copies(n, me, -1, send, recv, ssem, rsem)
    for copy in copies:
        copy.start()
    change = []
    key_part = []
    for b in range(blocks):
        rows = pl.ds(b * BLK, BLK)
        cumulative, middle, _ = decays(g_ref, rows)
        query = q_ref[rows, :].astype(jnp.float32) * scale
        key = k_ref[rows, :].astype(jnp.float32)
        value = v_ref[rows, :]
        d_out = d_ref[rows, :]
        rise, fall = jnp.exp(cumulative - middle), jnp.exp(middle - cumulative)
        lifted_q = (query * rise).astype(jnp.bfloat16)
        lifted_k = (key * fall).astype(jnp.bfloat16)
        scores = jnp.where(causal, mm(lifted_q, lifted_k, NT), 0.0).astype(jnp.bfloat16)
        d_scores = jnp.where(causal, mm(d_out, value, NT), 0.0).astype(jnp.bfloat16)
        d_lifted_q = mm(d_scores, lifted_k, NN)
        d_lifted_k = mm(d_scores, lifted_q, TN)
        grown = jnp.exp(cumulative)
        d_carried = mm(d_out, states_ref[b], NN) * grown
        gq_ref[rows, :] = ((d_lifted_q * rise + d_carried) * scale).astype(jnp.bfloat16)
        change.append(
            lifted_q.astype(jnp.float32) * d_lifted_q
            - lifted_k.astype(jnp.float32) * d_lifted_k
            + query * d_carried
        )
        key_part.append(d_lifted_k * fall)
        gg_ref[rows, :] = change[b]
        gv_ref[rows, :] = mm(scores, d_out, TN).astype(gv_ref.dtype)
    collect(n, me, -1, copies, recv, total, width)
    for b in range(blocks):
        rows = pl.ds(b * BLK, BLK)
        cumulative, _, ending = decays(g_ref, rows)
        d_state = kept[b] + total[...] * jnp.exp(afters[b])
        d_rounded = d_state.astype(jnp.bfloat16)
        key = k_ref[rows, :].astype(jnp.float32)
        fade = jnp.exp(ending - cumulative)
        faded = key * fade
        d_faded = mm(v_ref[rows, :], d_rounded, NN)
        gk_ref[rows, :] = (key_part[b] + d_faded * fade).astype(jnp.bfloat16)
        gv_ref[rows, :] = gv_ref[rows, :] + mm(faded.astype(jnp.bfloat16), d_rounded, NT)
        moved = faded * d_faded
        at_end = jnp.sum(moved, axis=0, keepdims=True) + jnp.exp(ending) * jnp.sum(
            states_ref[b].astype(jnp.float32) * d_state, axis=0, keepdims=True
        )
        gg_ref[rows, :] = block_sums(triangle(False), gg_ref[rows, :] - moved) + at_end


def exchange_scratch(n, blocks, width, channels):
    return [
        pltpu.VMEM((blocks, width, channels), jnp.float32),
        pltpu.VMEM((width, channels), jnp.float32),
        pltpu.VMEM((width + 16, channels), jnp.bfloat16),
        pltpu.VMEM((n - 1, width + 16, channels), jnp.bfloat16),
        pltpu.SemaphoreType.DMA((n - 1,)),
        pltpu.SemaphoreType.DMA((n - 1,)),
    ]


def in_vmem(count):
    return [pl.BlockSpec(memory_space=pltpu.VMEM)] * count


def mixer_forward(q, k, v, g, scale):
    n = lax.axis_size("sp")
    length, channels = q.shape
    width = v.shape[1]
    blocks = length // BLK
    return pl.pallas_call(
        functools.partial(forward_kernel, n, scale),
        out_shape=(
            jax.ShapeDtypeStruct((length, width), jnp.bfloat16),
            jax.ShapeDtypeStruct((blocks, width, channels), jnp.bfloat16),
        ),
        in_specs=in_vmem(4),
        out_specs=tuple(in_vmem(2)),
        scratch_shapes=exchange_scratch(n, blocks, width, channels),
        compiler_params=pltpu.CompilerParams(
            collective_id=1, has_side_effects=True, vmem_limit_bytes=16 * 1024 * 1024
        ),
        cost_estimate=pl.CostEstimate(
            flops=4_000_000_000, bytes_accessed=4 * length * width, transcendentals=0
        ),
        name="mixer_forward",
    )(q, k, v, g)


def mixer_backward(q, k, v, g, d, states, scale):
    n = lax.axis_size("sp")
    length, channels = q.shape
    width = v.shape[1]
    blocks = length // BLK
    return pl.pallas_call(
        functools.partial(backward_kernel, n, scale),
        out_shape=(
            jax.ShapeDtypeStruct((length, channels), jnp.bfloat16),
            jax.ShapeDtypeStruct((length, channels), jnp.bfloat16),
            jax.ShapeDtypeStruct((length, width), jnp.float32),
            jax.ShapeDtypeStruct((length, channels), jnp.float32),
        ),
        in_specs=in_vmem(6),
        out_specs=tuple(in_vmem(4)),
        scratch_shapes=exchange_scratch(n, blocks, width, channels),
        compiler_params=pltpu.CompilerParams(
            collective_id=2, has_side_effects=True, vmem_limit_bytes=16 * 1024 * 1024
        ),
        cost_estimate=pl.CostEstimate(
            flops=8_000_000_000, bytes_accessed=4 * length * width, transcendentals=0
        ),
        name="mixer_backward",
    )(q, k, v, g, d, states)


def expert_pass(rows_in, routed_rows, gate_w, up_w, down_w):
    gate_pre = jnp.dot(rows_in, gate_w, preferred_element_type=jnp.float32)
    up_pre = jnp.dot(rows_in, up_w, preferred_element_type=jnp.float32)
    sigmoid_gate = jax.nn.sigmoid(gate_pre)
    active = gate_pre * sigmoid_gate
    hidden = (active * up_pre).astype(jnp.bfloat16)
    d_hidden = lax.dot_general(
        routed_rows, down_w, (((1,), (1,)), ((), ())), preferred_element_type=jnp.float32
    )
    d_gate = (d_hidden * up_pre * sigmoid_gate * (1.0 + gate_pre * (1.0 - sigmoid_gate))).astype(
        jnp.bfloat16
    )
    d_up = (d_hidden * active).astype(jnp.bfloat16)
    rows_first = (((0,), (0,)), ((), ()))
    grad_gate = lax.dot_general(
        rows_in, d_gate, rows_first, preferred_element_type=jnp.float32
    ).astype(jnp.bfloat16)
    grad_up = lax.dot_general(rows_in, d_up, rows_first, preferred_element_type=jnp.float32).astype(
        jnp.bfloat16
    )
    grad_down = lax.dot_general(
        hidden, routed_rows, rows_first, preferred_element_type=jnp.float32
    ).astype(jnp.bfloat16)
    return (grad_gate, grad_up, grad_down, d_gate, d_up)


def local(
    d_out,
    route_expert,
    route_weight,
    expert_inputs,
    w_gate,
    w_up,
    w_down,
    w_out,
    queries,
    keys,
    values,
    log_decay,
):
    tok_rows = d_out.shape[0]
    model_width = d_out.shape[1]
    experts = lax.axis_size("sp")
    capacity = expert_inputs.shape[1] // experts
    flat_experts = route_expert.reshape(-1)
    onehot = (flat_experts[:, None] == jnp.arange(experts, dtype=jnp.int32)[None, :]).astype(
        jnp.int32
    )
    before = jnp.cumsum(onehot, axis=0) - onehot
    rank_slot = jnp.sum(before * onehot, axis=1)
    slot_index = flat_experts * capacity + rank_slot
    quarter = model_width // lax.axis_size("tp")
    column_start = lax.axis_index("tp") * quarter
    own_cols = lax.dynamic_slice_in_dim(d_out, column_start, quarter, 1)
    scaled = (
        jnp.repeat(own_cols, 2, axis=0).astype(jnp.float32) * route_weight.reshape(-1)[:, None]
    ).astype(jnp.bfloat16)
    outbox = (
        jnp.zeros((experts * capacity, own_cols.shape[1]), jnp.bfloat16).at[slot_index].set(scaled)
    )
    outbox = outbox.reshape(experts, capacity, own_cols.shape[1])
    partial_rows = lax.all_to_all(outbox, "sp", split_axis=0, concat_axis=0, tiled=True)
    routed = lax.all_gather(partial_rows, "tp", axis=2, tiled=True)
    routed = routed.reshape(experts * capacity, model_width)
    rows_in = expert_inputs[0]
    gate_w = w_gate[0]
    up_w = w_up[0]
    grad_gate, grad_up, grad_down, d_gate, d_up = expert_pass(
        rows_in, routed, gate_w, up_w, w_down[0]
    )
    partial_terms = lax.dot_general(
        d_gate, gate_w, (((1,), (1,)), ((), ())), preferred_element_type=jnp.float32
    )
    partial_terms = partial_terms + lax.dot_general(
        d_up, up_w, (((1,), (1,)), ((), ())), preferred_element_type=jnp.float32
    )
    rounded = lax.optimization_barrier(partial_terms.astype(jnp.bfloat16)).astype(jnp.float32)
    summed = lax.psum_scatter(rounded.astype(jnp.bfloat16), "tp", scatter_dimension=1, tiled=True)
    returned = lax.all_to_all(
        summed.reshape(experts, capacity, quarter), "sp", split_axis=0, concat_axis=0, tiled=True
    )
    picked = returned.reshape(experts * capacity, quarter)[slot_index].astype(jnp.float32)
    picked = picked.reshape(tok_rows, 2, quarter).sum(axis=1)
    mix_cols = (own_cols.astype(jnp.float32) + picked).astype(jnp.bfloat16)
    mix_grad = lax.all_gather(mix_cols, "tp", axis=1, tiled=True)
    scale_q = queries.shape[2] ** (-0.5)
    q, k, v, g = queries[:, 0], keys[:, 0], values[:, 0], log_decay[:, 0]
    mixed, states = mixer_forward(q, k, v, g, scale_q)
    grad_proj = lax.psum_scatter(
        lax.dot_general(
            mix_grad, mixed, (((0,), (0,)), ((), ())), preferred_element_type=jnp.float32
        ).astype(jnp.bfloat16),
        "sp",
        scatter_dimension=0,
        tiled=True,
    ).astype(jnp.float32)
    d_mixed = jnp.dot(mix_grad, w_out, preferred_element_type=jnp.float32).astype(jnp.bfloat16)
    grad_q, grad_k, grad_v, grad_g = mixer_backward(q, k, v, g, d_mixed, states, scale_q)
    return (
        grad_gate[None],
        grad_up[None],
        grad_down[None],
        grad_proj,
        grad_q[:, None],
        grad_k[:, None],
        grad_v.astype(jnp.bfloat16)[:, None],
        grad_g[:, None],
    )


def solution(mesh):
    return jax.shard_map(
        local,
        mesh=mesh,
        in_specs=(
            P("sp", None),
            P("sp", None),
            P("sp", None),
            P("sp", None, None),
            P("sp", None, "tp"),
            P("sp", None, "tp"),
            P("sp", "tp", None),
            P(None, "tp"),
            P("sp", "tp", None),
            P("sp", "tp", None),
            P("sp", "tp", None),
            P("sp", "tp", None),
        ),
        out_specs=(
            P("sp", None, "tp"),
            P("sp", None, "tp"),
            P("sp", "tp", None),
            P("sp", "tp"),
            P("sp", "tp", None),
            P("sp", "tp", None),
            P("sp", "tp", None),
            P("sp", "tp", None),
        ),
        check_vma=False,
    )
```

time: 444 us -> 331 us (0.75)
  waiting for transfers between devices: 42.7 us -> 131 us
  blocking collectives: 121 us -> 36.3 us
  other arithmetic: 87.5 us -> 20.2 us
  local copies, waits for them, and re-layouts: 60.6 us -> 17.9 us
  matrix products: 104 us -> 61.4 us
  Pallas kernels: 0 us -> 39.6 us
    all_gather x3 -> x0, blocking collectives: 84.4 us -> none  [carried_in(): lax.all_gather(part.astype(kind), axis)]
    reduce_scatter x1, waiting for transfers between devices: 0.01 us -> 48 us  [local(): lax.psum_scatter(rounded.astype(jnp.bfloat16), 'tp', scatter_dimension=1,...]
    dot_general x74 -> x0, matrix products: 41.3 us -> none  [the longest x24 15.7 us: advance(): jnp.einsum('hij,hje->hie', scores, value_block, precision=precise)]
    pallas_call x0 -> x2, Pallas kernels: none -> 39.6 us  [the longest x1 26.2 us: mixer_backward(): pl.pallas_call(functools.partial(backward_kernel, n, scale), out_shape=(j...]
    dot_general x24 -> x0, other arithmetic: 36 us -> none  [advance(): jnp.einsum('hid,hjd,hijd->hij', query_block, key_block, within, precision...]
    reduce_scatter x1, waiting for transfers between devices: 0.01 us -> 34.5 us  [local(): lax.psum_scatter(lax.dot_general(mix_grad, mixed, (((0,), (0,)), ((), ())...]
    squeeze x48 -> x0, local copies, waits for them, and re-layouts: 18.5 us -> none  [the longest x32 18.4 us: block_mixer(): lax.scan(jax.checkpoint(advance), initial, (to_blocks(scaled_queries), to...]
    reduce_sum x24 -> x0, other arithmetic: 17.7 us -> none  [the longest x8 17 us: advance(): cumulative[:, :, None, :] - cumulative[:, None, :, :]]
  transfers between devices with their start and end apart: 5 -> 5, of which waited for: 2 -> 4; matrix products, arithmetic and copies ran while one was open for 45% -> 12% of each run, Pallas kernels for 0% -> 12%
where the time goes in v1:
time: 331 us; the launch traced here: 326 us
  waiting for transfers between devices  131 us (40%)
  matrix products  61.4 us (19%)
  Pallas kernels  39.6 us (12%)
  blocking collectives  36.3 us (11%)
  other arithmetic  20.2 us (6%)
  local copies, waits for them, and re-layouts  17.9 us (5%)
  between operations  14.6 us (4%)
  starting transfers between devices  5.85 us (2%)
    reduce_scatter x1, waiting for transfers between devices, local(): lax.psum_scatter(rounded.astype(jnp.bfloat16), 'tp', scatter_dimension=1,...  48 us
    all_to_all x1, blocking collectives, local(): lax.all_to_all(outbox, 'sp', split_axis=0, concat_axis=0, tiled=True)  36.3 us
    reduce_scatter x1, waiting for transfers between devices, local(): lax.psum_scatter(lax.dot_general(mix_grad, mixed, (((0,), (0,)), ((), ())...  34.5 us
    all_to_all x1, waiting for transfers between devices, local(): lax.all_to_all(summed.reshape(experts, capacity, quarter), 'sp', split_ax...  28.4 us
    pallas_call x1, Pallas kernels, mixer_backward(): pl.pallas_call(functools.partial(backward_kernel, n, scale), out_shape=(j...  26.2 us
    all_gather x1, waiting for transfers between devices, local(): routed = lax.all_gather(partial_rows, 'tp', axis=2, tiled=True)  19.7 us
    pallas_call x1, Pallas kernels, mixer_forward(): pl.pallas_call(functools.partial(forward_kernel, n, scale), out_shape=(ja...  13.5 us
    dot_general x1, matrix products, expert_pass(): lax.dot_general(routed_rows, down_w, (((1,), (1,)), ((), ())), preferred_...  9.72 us
  transfers between devices with their start and end apart: 5, of which 4 were waited for; matrix products, arithmetic and copies ran while one was open for 12% of the time, Pallas kernels for 12%

profile of v1, /device:TPU:0, one launch (start us, length us, event | category | flops | bytes accessed | tf_op | source)
XLA Modules:
  0.0 326.4 jit_solution(9267400011580704838)
XLA Ops:
  9.6 2.3 reduce-window.6
  15.6 3.7 %convert_element_type.72 = f32[1024,512]{1,0:T(8,128)} reshape(f32[512,2,512]{2,1,0:T(2,128)} %broadcast_in_dim.31) | data formatting | bytes 4194304 | tf_op jit(solution)/shard_map/convert_element_type | solution.py:337
  19.6 7.2 %scatter_custom_fusion = bf16[1152,512]{1,0:T(8,128)(2,1)} fusion(s32[1024]{0:T(1024)S(1)} %bitcast.103, f32[1024,512]{1,0:T(8,128)} %convert_element_type.72, f32[1024]{0:T(1024)S(1)} %mul.58, bf16[]{:T(256)} %constant.9.clone.1), kind=kCustom, calls=%fused_computation.32 | custom fusion | flops 1048576 | bytes 3280898 | tf_op jit(solution)/shard_map/scatter | solution.py:340
  26.9 36.3 %all_to_all.10 = bf16[8,144,512]{2,1,0:T(8,128)(2,1)} all-to-all(bf16[8,144,512]{2,1,0:T(8,128)(2,1)} %bitcast.100), channel_id=1, replica_groups=mesh['sp'=8,'tp'=4] {'sp'}, dimensions={0} | all-to-all | bytes 2359296 | tf_op jit(solution)/shard_map/all_to_all | solution.py:343
  63.5 8.2 %fusion.4 = f32[1152,704]{0,1:T(8,128)} fusion(bf16[1,1152,2048]{2,1,0:T(8,128)(2,1)} %param.15, bf16[1,2048,704]{1,2,0:T(8,128)(2,1)S(1)} %copy-done), kind=kOutput, calls=%fused_computation.7 | convolution fusion | flops 3321888768 | bytes 10846208 | tf_op jit(solution)/shard_map/dot_general | solution.py:283
  71.6 8.1 %fusion.6 = f32[1152,704]{0,1:T(8,128)} fusion(bf16[1,1152,2048]{2,1,0:T(8,128)(2,1)} %param.15, bf16[1,2048,704]{1,2,0:T(8,128)(2,1)S(1)} %copy-done.12), kind=kOutput, calls=%fused_computation.9 | convolution fusion | flops 3321888768 | bytes 10846208 | tf_op jit(solution)/shard_map/dot_general | solution.py:284
  79.7 19.7 %all-gather.3.cloned.1.call-done = bf16[8,144,2048]{2,1,0:T(8,128)(2,1)} async-done(((bf16[8,144,512]{2,1,0:T(8,128)(2,1)}), bf16[8,144,2048]{2,1,0:T(8,128)(2,1)}) %all-gather.3.cloned.1.call-update) | async-done | bytes 4718608 | tf_op jit(solution)/shard_map/all_gather | solution.py:344
  99.5 9.7 %multiply_convert_fusion.1 = (bf16[1152,704]{0,1:T(8,128)(2,1)S(1)}, bf16[1152,704]{0,1:T(8,128)(2,1)S(1)}) fusion(f32[1152,704]{0,1:T(8,128)} %fusion.4, f32[1152,704]{0,1:T(8,128)} %fusion.6, bf16[1152,2048]{1,0:T(8,128)(2,1)} %bitcast.106, bf16[1,704,2048]{2,1,0:T(8,128)(2,1)} %param.18), kind=kOutput, calls=%fused_computation.15 | convolution fusion | flops 3332431872 | bytes 17334272 | tf_op jit(solution)/shard_map/dot_general | solution.py:288
  109.2 4.2 %fusion.22 = f32[1152,2048]{1,0:T(8,128)S(1)} fusion(bf16[1152,704]{0,1:T(8,128)(2,1)S(1)} %get-tuple-element.37, bf16[1,2048,704]{1,2,0:T(8,128)(2,1)S(1)} %copy-done), kind=kOutput, calls=%fused_computation.22 | convolution fusion | flops 3321888768 | bytes 13942784 | tf_op jit(solution)/shard_map/dot_general | solution.py:352
  113.4 5.6 %add_convert_fusion = bf16[1152,2048]{1,0:T(8,128)(2,1)} fusion(f32[1152,2048]{1,0:T(8,128)S(1)} %fusion.22, bf16[1152,704]{0,1:T(8,128)(2,1)S(1)} %get-tuple-element.36, bf16[1,2048,704]{1,2,0:T(8,128)(2,1)S(1)} %copy-done.13), kind=kOutput, calls=%fused_computation.2 | convolution fusion | flops 3326607360 | bytes 18661376 | tf_op jit(solution)/shard_map/dot_general | solution.py:355
  119.0 48.0 %reduce-scatter.3.cloned.1.call-done = bf16[1152,512]{1,0:T(8,128)(2,1)} async-done(((bf16[1152,2048]{1,0:T(8,128)(2,1)}), bf16[1152,512]{1,0:T(8,128)(2,1)}) %reduce-scatter.3.cloned.1.call-update) | async-done | bytes 1179664 | tf_op jit(solution)/shard_map/reduce_scatter | solution.py:359
  167.0 5.5 %all-to-all-start.1 = ((bf16[8,144,512]{2,1,0:T(8,128)(2,1)}), bf16[8,144,512]{2,1,0:T(8,128)(2,1)S(1)}, u32[]{:S(2)}, u32[]{:S(2)}) async-start(bf16[8,144,512]{2,1,0:T(8,128)(2,1)} %bitcast.101), calls=%async_computation.2 | async-start | bytes 2359296 | tf_op jit(solution)/shard_map/all_to_all | solution.py:360
  172.6 28.4 %all-to-all-done.1 = bf16[8,144,512]{2,1,0:T(8,128)(2,1)S(1)} async-done(((bf16[8,144,512]{2,1,0:T(8,128)(2,1)}), bf16[8,144,512]{2,1,0:T(8,128)(2,1)S(1)}, u32[]{:S(2)}, u32[]{:S(2)}) %all-to-all-start.1) | async-done | bytes 1179680 | tf_op jit(solution)/shard_map/all_to_all | solution.py:360
  200.9 5.1 %gather_fusion = bf16[1024,512]{1,0:T(8,128)(2,1)} fusion(bf16[1152,512]{1,0:T(8,128)(2,1)S(1)} %bitcast.99, s32[1024]{0:T(1024)S(1)} %broadcast_clamp_fusion), kind=kCustom, calls=%fused_computation | custom fusion | bytes 2101248 | tf_op jit(solution)/shard_map/gather | solution.py:363
  206.0 2.4 reshape.86
  208.4 3.7 %reduce_sum.22 = f32[512,512]{1,0:T(8,128)} reduce(f32[512,2,512]{2,1,0:T(2,128)S(1)} %reshape.86, f32[]{:T(128)} %constant.24.clone.1), dimensions={1}, to_apply=%region_5.6 | reduce | flops 262144 | bytes 3145732 | tf_op jit(solution)/shard_map/reduce_sum | solution.py:364
  212.1 2.3 add_convert_fusion.1
  214.6 13.5 %mixer_forward.1 = (bf16[512,256]{1,0:T(8,128)(2,1)S(1)}, bf16[8,256,128]{2,1,0:T(8,128)(2,1)S(1)}) custom-call(bf16[512,128]{1,0:T(8,128)(2,1)S(1)} %bitcast.95, bf16[512,128]{1,0:T(8,128)(2,1)S(1)} %bitcast.97, bf16[512,256]{1,0:T(8,128)(2,1)S(1)} %bitcast.91, f32[512,128]{1,0:T(8,128)S(1)} %bitcast.93), custom_call_target="tpu_custom_call" | custom-call | flops 4000000000 | bytes 524288 | tf_op jit(solution)/shard_map/mixer_forward/pallas_call | solution.py:237
  228.1 7.8 %fusion.19 = bf16[1,2048,704]{1,2,0:T(8,128)(2,1)} fusion(bf16[1152,704]{0,1:T(8,128)(2,1)S(1)} %copy-done.17, bf16[1,1152,2048]{2,1,0:T(8,128)(2,1)} %param.15), kind=kOutput, calls=%fused_computation.21 | convolution fusion | flops 3323330560 | bytes 9224192 | tf_op jit(solution)/shard_map/dot_general | solution.py:296
  236.0 5.4 %fusion.15 = bf16[1,704,2048]{2,1,0:T(8,128)(2,1)} fusion(bf16[1152,2048]{1,0:T(8,128)(2,1)S(1)} %bitcast.109, f32[1152,704]{0,1:T(8,128)S(1)} %copy-done.19, f32[1152,704]{0,1:T(8,128)S(1)} %copy-done.18), kind=kOutput, calls=%fused_computation.19 | convolution fusion | flops 3328196608 | bytes 14090240 | tf_op jit(solution)/shard_map/dot_general | solution.py:302
  241.3 3.3 %convolution_convert_fusion.1 = bf16[2048,256]{1,0:T(8,128)(2,1)} fusion(bf16[512,2048]{1,0:T(8,128)(2,1)} %all-gather.5.cloned.1.call-done, bf16[512,256]{1,0:T(8,128)(2,1)S(1)} %get-tuple-element.14), kind=kOutput, calls=%fused_computation.29 | convolution fusion | flops 537395200 | bytes 3407872 | tf_op jit(solution)/shard_map/dot_general | solution.py:371
  244.7 8.4 %fusion.16 = bf16[1,2048,704]{1,2,0:T(8,128)(2,1)} fusion(bf16[1152,704]{0,1:T(8,128)(2,1)} %copy-done.20, bf16[1,1152,2048]{2,1,0:T(8,128)(2,1)} %param.15), kind=kOutput, calls=%fused_computation.20 | convolution fusion | flops 3323330560 | bytes 9224192 | tf_op jit(solution)/shard_map/dot_general | solution.py:299
  254.4 26.2 %mixer_backward.1 = (bf16[512,128]{1,0:T(8,128)(2,1)S(1)}, bf16[512,128]{1,0:T(8,128)(2,1)S(1)}, f32[512,256]{1,0:T(8,128)S(1)}, f32[512,128]{1,0:T(8,128)S(1)}) custom-call(bf16[512,128]{1,0:T(8,128)(2,1)S(1)} %bitcast.96, bf16[512,128]{1,0:T(8,128)(2,1)S(1)} %bitcast.98, bf16[512,256]{1,0:T(8,128)(2,1)S(1)} %bitcast.92, f32[512,128]{1,0:T(8,128)S(1)} %bitcast.94, ...), custom_call_target="tpu_custom_call" | custom-call | flops 8000000000 | bytes 524288 | tf_op jit(solution)/shard_map/mixer_backward/pallas_call | solution.py:261
  281.3 34.5 %reduce-scatter.5.cloned.1.call-done = bf16[256,256]{1,0:T(8,128)(2,1)} async-done(((bf16[2048,256]{1,0:T(8,128)(2,1)}), bf16[256,256]{1,0:T(8,128)(2,1)}) %reduce-scatter.5.cloned.1.call-update) | async-done | bytes 131088 | tf_op jit(solution)/shard_map/reduce_scatter | solution.py:370
  (79 shorter events, 12.5 us)
Async XLA Ops:
  7.2 56.3 %copy-start = (bf16[1,2048,704]{1,2,0:T(8,128)(2,1)S(1)}, bf16[1,2048,704]{1,2,0:T(8,128)(2,1)}, u32[]{:S(2)}) copy-start(bf16[1,2048,704]{1,2,0:T(8,128)(2,1)} %param.16) | copy-start | bytes 8650756
  7.2 92.3 %all-gather.3.cloned.1.call-start = ((), (), s32[]{:S(2)}) async-start(), calls=%async_computation.4 | async-start | bytes 5898240 | tf_op jit(solution)/shard_map/all_gather | solution.py:344
  15.6 3.7 %copy-start.11 = (f32[512,2]{0,1:T(2,128)S(1)}, f32[512,2]{0,1:T(2,128)}, u32[]{:S(2)}) copy-start(f32[512,2]{0,1:T(2,128)} %param.14) | copy-start | bytes 12292
  63.2 103.8 %reduce-scatter.3.cloned.1.call-start = ((), (), s32[]{:S(2)}) async-start(), calls=%async_computation.5 | async-start | bytes 5898240 | tf_op jit(solution)/shard_map/reduce_scatter | solution.py:359
  63.4 8.2 %copy-start.12 = (bf16[1,2048,704]{1,2,0:T(8,128)(2,1)S(1)}, bf16[1,2048,704]{1,2,0:T(8,128)(2,1)}, u32[]{:S(2)}) copy-start(bf16[1,2048,704]{1,2,0:T(8,128)(2,1)} %param.17) | copy-start | bytes 8650756
  109.2 4.2 %copy-start.16 = (bf16[1152,704]{0,1:T(8,128)(2,1)}, bf16[1152,704]{0,1:T(8,128)(2,1)S(1)}, u32[]{:S(2)}) copy-start(bf16[1152,704]{0,1:T(8,128)(2,1)S(1)} %get-tuple-element.37) | copy-start | bytes 4866052
  109.2 4.2 %copy-start.20 = (bf16[1152,704]{0,1:T(8,128)(2,1)}, bf16[1152,704]{0,1:T(8,128)(2,1)S(1)}, u32[]{:S(2)}) copy-start(bf16[1152,704]{0,1:T(8,128)(2,1)S(1)} %get-tuple-element.36) | copy-start | bytes 4866052
  109.2 4.2 %copy-start.13 = (bf16[1,2048,704]{1,2,0:T(8,128)(2,1)S(1)}, bf16[1,2048,704]{1,2,0:T(8,128)(2,1)}, u32[]{:S(2)}) copy-start(bf16[1,2048,704]{1,2,0:T(8,128)(2,1)} %param.17) | copy-start | bytes 8650756
  167.0 33.9 %all-to-all-start.1 = ((bf16[8,144,512]{2,1,0:T(8,128)(2,1)}), bf16[8,144,512]{2,1,0:T(8,128)(2,1)S(1)}, u32[]{:S(2)}, u32[]{:S(2)}) async-start(bf16[8,144,512]{2,1,0:T(8,128)(2,1)} %bitcast.101), calls=%async_computation.2 | async-start | bytes 2359296 | tf_op jit(solution)/shard_map/all_to_all | solution.py:360
  172.5 68.8 %all-gather.5.cloned.1.call-start = ((), (), s32[]{:S(2)}) async-start(), calls=%async_computation.6 | async-start | bytes 2621440 | tf_op jit(solution)/shard_map/all_gather | solution.py:366
  208.4 6.1 %copy-start.2 = (bf16[512,1,256]{2,0,1:T(8,128)(2,1)S(1)}, bf16[512,1,256]{2,0,1:T(8,128)(2,1)}, u32[]{:S(2)}) copy-start(bf16[512,1,256]{2,0,1:T(8,128)(2,1)} %param.22) | copy-start | bytes 786436
  208.4 6.1 %copy-start.4 = (f32[512,1,128]{2,1,0:T(1,128)S(1)}, f32[512,1,128]{2,1,0:T(1,128)}, u32[]{:S(2)}) copy-start(f32[512,1,128]{2,1,0:T(1,128)} %param.23) | copy-start | bytes 786436
  208.4 6.1 %copy-start.6 = (bf16[512,1,128]{2,0,1:T(8,128)(2,1)S(1)}, bf16[512,1,128]{2,0,1:T(8,128)(2,1)}, u32[]{:S(2)}) copy-start(bf16[512,1,128]{2,0,1:T(8,128)(2,1)} %param.20) | copy-start | bytes 393220
  208.4 6.1 %copy-start.7 = (bf16[512,1,128]{2,0,1:T(8,128)(2,1)S(1)}, bf16[512,1,128]{2,0,1:T(8,128)(2,1)}, u32[]{:S(2)}) copy-start(bf16[512,1,128]{2,0,1:T(8,128)(2,1)} %param.21) | copy-start | bytes 393220
  214.5 101.3 %reduce-scatter.5.cloned.1.call-start = ((), (), s32[]{:S(2)}) async-start(), calls=%async_computation.7 | async-start | bytes 1179648 | tf_op jit(solution)/shard_map/reduce_scatter | solution.py:370
  214.6 13.5 %copy-start.17 = (bf16[1152,704]{0,1:T(8,128)(2,1)S(1)}, bf16[1152,704]{0,1:T(8,128)(2,1)}, u32[]{:S(2)}) copy-start(bf16[1152,704]{0,1:T(8,128)(2,1)} %copy-done.16) | copy-start | bytes 4866052
  214.6 21.4 %slice-start = ((s8[4718592]{0:T(1024)(128)(4,1)}), s8[4194304]{0:T(1024)(128)(4,1)S(1)}, s32[]{:S(2)}) async-start(s8[4718592]{0:T(1024)(128)(4,1)} %bitcast.107), calls=%async_computation.8 | async-start | bytes 8388608
  228.1 7.9 %copy-start.9 = (bf16[8,256,128]{2,1,0:T(8,128)(2,1)}, bf16[8,256,128]{2,1,0:T(8,128)(2,1)S(1)}, u32[]{:S(2)}) copy-start(bf16[8,256,128]{2,1,0:T(8,128)(2,1)S(1)} %get-tuple-element.15.states_ref) | copy-start | bytes 1572868
  228.1 7.9 %slice-start.1 = ((s8[4718592]{0:T(1024)(128)(4,1)}), s8[524288]{0:T(1024)(128)(4,1)S(1)}, s32[]{:S(2)}) async-start(s8[4718592]{0:T(1024)(128)(4,1)} %bitcast.107), calls=%async_computation.9 | async-start | bytes 1048576
  228.1 7.8 %copy-start.18 = (f32[1152,704]{0,1:T(8,128)S(1)}, f32[1152,704]{0,1:T(8,128)}, u32[]{:S(2)}) copy-start(f32[1152,704]{0,1:T(8,128)} %fusion.4) | copy-start | bytes 9732100
  228.1 7.8 %copy-start.19 = (f32[1152,704]{0,1:T(8,128)S(1)}, f32[1152,704]{0,1:T(8,128)}, u32[]{:S(2)}) copy-start(f32[1152,704]{0,1:T(8,128)} %fusion.6) | copy-start | bytes 9732100
  244.7 8.5 %copy-start.14 = (bf16[512,2048]{1,0:T(8,128)(2,1)S(1)}, bf16[512,2048]{1,0:T(8,128)(2,1)}, u32[]{:S(2)}) copy-start(bf16[512,2048]{1,0:T(8,128)(2,1)} %all-gather.5.cloned.1.call-done) | copy-start | bytes 6291460
  244.7 8.5 %copy-start.15 = (bf16[2048,256]{1,0:T(8,128)(2,1)S(1)}, bf16[2048,256]{1,0:T(8,128)(2,1)}, u32[]{:S(2)}) copy-start(bf16[2048,256]{1,0:T(8,128)(2,1)} %param.19) | copy-start | bytes 3145732
  254.4 65.0 %copy-start.1 = (bf16[1,2048,704]{1,2,0:T(8,128)(2,1)S(1)}, bf16[1,2048,704]{1,2,0:T(8,128)(2,1)}, u32[]{:S(2)}) copy-start(bf16[1,2048,704]{1,2,0:T(8,128)(2,1)} %param.16) | copy-start | bytes 8650756
  (4 other events, 4.4 us)
Sparse Core Ops, SparseCore 0:
  63.3 36.0 all-gather.2
  119.2 47.7 reduce-scatter.2
  214.6 20.6 all-gather.4
  244.8 70.9 reduce-scatter.4

commit v2 on v1

--- a/solution.py
+++ b/solution.py
@@ -42,13 +42,119 @@
     return cumulative, middle, ending
 
 
-def greet(n, me):
+def greet(n, me, tp=None):
     barrier = pltpu.get_barrier_semaphore()
+    others = [{"sp": lax.rem(me + k, n)} for k in range(1, n)]
+    if tp is not None:
+        others += [{"tp": other} for other in tp]
+    for other in others:
+        pl.semaphore_signal(barrier, inc=1, device_id=other, device_id_type=MESH)
+    return barrier, len(others)
+
+
+def route_kernel(n, cap, d_ref, expert_ref, weight_ref, arrived_ref, slot_ref, outbox, ssem, rsem, lsem):
+    me = lax.axis_index("sp")
+    barrier, greeted = greet(n, me)
+    tokens = d_ref.shape[0]
+    quarter = outbox.shape[2]
+    start = pl.multiple_of(lax.axis_index("tp") * quarter, quarter)
+    own = d_ref[:, pl.ds(start, quarter)].astype(jnp.float32)
+    kinds = lax.broadcasted_iota(jnp.int32, (n, tokens), 0)
+    named = [(kinds == expert_ref[j : j + 1, :]).astype(jnp.float32) for j in range(2)]
+    earlier = lax.broadcasted_iota(jnp.int32, (tokens, tokens), 0) < lax.broadcasted_iota(
+        jnp.int32, (tokens, tokens), 1
+    )
+    before = mm((named[0] + named[1]).astype(jnp.bfloat16), earlier.astype(jnp.bfloat16), NN)
+    scaled = []
+    slots = []
+    for j in range(2):
+        rank = jnp.sum(before * named[j], axis=0, keepdims=True).astype(jnp.int32)
+        slots.append(expert_ref[j : j + 1, :] * cap + rank)
+        slot_ref[j : j + 1, :] = slots[j]
+        scaled.append((own * weight_ref[:, j : j + 1]).astype(jnp.bfloat16))
+    places = lax.broadcasted_iota(jnp.int32, (cap, tokens), 0)
+    for e in range(n):
+        rows = jnp.zeros((cap, quarter), jnp.float32)
+        for j in range(2):
+            picks = (slots[j] - e * cap == places).astype(jnp.float32).astype(jnp.bfloat16)
+            rows = rows + mm(picks, scaled[j], NN)
+        outbox[e] = rows.astype(jnp.bfloat16)
+    pl.semaphore_wait(barrier, greeted)
+    exchange(n, me, outbox, arrived_ref, ssem, rsem, lsem)
+
+
+def exchange(n, me, source, target, ssem, rsem, lsem):
+    copies = []
     for k in range(1, n):
-        pl.semaphore_signal(
-            barrier, inc=1, device_id={"sp": lax.rem(me + k, n)}, device_id_type=MESH
+        peer = lax.rem(me + k, n)
+        copies.append(
+            pltpu.make_async_remote_copy(
+                src_ref=source.at[peer],
+                dst_ref=target.at[me],
+                send_sem=ssem.at[k - 1],
+                recv_sem=rsem.at[k - 1],
+                device_id={"sp": peer},
+                device_id_type=MESH,
+            )
         )
-    return barrier
+    for copy in copies:
+        copy.start()
+    stays = pltpu.make_async_copy(source.at[me], target.at[me], lsem)
+    stays.start()
+    stays.wait()
+    for copy in copies:
+        copy.wait()
+
+
+def return_kernel(
+    n, tp, cap, sums_ref, slot_ref, d_ref, gathered_ref, back, ssem, rsem, lsem, tsend, trecv
+):
+    me = lax.axis_index("sp")
+    col = lax.axis_index("tp")
+    partner = col + 1 - 2 * lax.rem(col, 2)
+    far = [lax.rem(col + 2 * s, tp) for s in range(1, tp // 2)]
+    barrier, greeted = greet(n, me, [partner] + far)
+    pl.semaphore_wait(barrier, greeted)
+    exchange(n, me, sums_ref, back, ssem, rsem, lsem)
+    tokens = d_ref.shape[0]
+    quarter = back.shape[2]
+    start = pl.multiple_of(col * quarter, quarter)
+    places = lax.broadcasted_iota(jnp.int32, (cap, tokens), 0)
+    picked = jnp.zeros((tokens, quarter), jnp.float32)
+    for e in range(n):
+        here = jnp.zeros((cap, tokens), jnp.float32)
+        for j in range(2):
+            here = here + (slot_ref[j : j + 1, :] - e * cap == places).astype(jnp.float32)
+        picked = picked + mm(here.astype(jnp.bfloat16), back[e], TN)
+    own = d_ref[:, pl.ds(start, quarter)].astype(jnp.float32)
+    gathered_ref[col] = (own + picked).astype(jnp.bfloat16)
+
+    def send(block, slot, target):
+        return pltpu.make_async_remote_copy(
+            src_ref=gathered_ref.at[block],
+            dst_ref=gathered_ref.at[block],
+            send_sem=tsend.at[slot],
+            recv_sem=trecv.at[slot],
+            device_id={"tp": target},
+            device_id_type=MESH,
+        )
+
+    across = [send(col, s + 1, far[s]) for s in range(len(far))]
+    beside = send(col, 0, partner)
+    for copy in across:
+        copy.start()
+    beside.start()
+    passed = []
+    for s in range(len(far)):
+        across[s].wait_recv()
+        block = lax.rem(col - 2 * (s + 1) + tp, tp)
+        passed.append(send(block, tp // 2 + s, partner))
+        passed[s].start()
+    for copy in across:
+        copy.wait_send()
+    beside.wait()
+    for copy in passed:
+        copy.wait()
 
 
 def state_copies(n, me, step, send_ref, recv_ref, send_sem, recv_sem):
@@ -82,7 +188,7 @@
     n, scale, q_ref, k_ref, v_ref, g_ref, mixed_ref, states_ref, kept, total, send, recv, ssem, rsem
 ):
     me = lax.axis_index("sp")
-    barrier = greet(n, me)
+    barrier, greeted = greet(n, me)
     length, width = v_ref.shape
     blocks = length // BLK
     causal = triangle(True)
@@ -101,7 +207,7 @@
         ahead = ahead + ending
     send[:width, :] = local.astype(jnp.bfloat16)
     send[width:, :] = jnp.broadcast_to(jnp.exp(ahead), (16, ahead.shape[1])).astype(jnp.bfloat16)
-    pl.semaphore_wait(barrier, n - 1)
+    pl.semaphore_wait(barrier, greeted)
     copies = state_copies(n, me, 1, send, recv, ssem, rsem)
     for copy in copies:
         copy.start()
@@ -132,25 +238,38 @@
     k_ref,
     v_ref,
     g_ref,
-    d_ref,
+    grad_ref,
+    w_ref,
+    mixed_ref,
     states_ref,
     gq_ref,
     gk_ref,
     gv_ref,
     gg_ref,
+    proj_ref,
     kept,
     total,
     send,
     recv,
     ssem,
     rsem,
+    d_ref,
+    part,
+    parts_in,
+    psend,
+    precv,
 ):
     me = lax.axis_index("sp")
-    barrier = greet(n, me)
+    barrier, greeted = greet(n, me)
     length, width = v_ref.shape
     blocks = length // BLK
     causal = triangle(True)
     local = jnp.zeros(total.shape, jnp.float32)
+    pieces, _, quarter = grad_ref.shape
+    d_mixed = jnp.zeros((length, width), jnp.float32)
+    for p in range(pieces):
+        d_mixed = d_mixed + mm(grad_ref[p], w_ref[p * quarter : (p + 1) * quarter, :], NN)
+    d_ref[...] = d_mixed.astype(jnp.bfloat16)
     after = jnp.zeros((1, q_ref.shape[1]), jnp.float32)
     afters = [None] * blocks
     for b in reversed(range(blocks)):
@@ -164,10 +283,30 @@
         after = after + ending
     send[:width, :] = local.astype(jnp.bfloat16)
     send[width:, :] = jnp.broadcast_to(jnp.exp(after), (16, after.shape[1])).astype(jnp.bfloat16)
-    pl.semaphore_wait(barrier, n - 1)
+    pl.semaphore_wait(barrier, greeted)
     copies = state_copies(n, me, -1, send, recv, ssem, rsem)
     for copy in copies:
         copy.start()
+    share = part.shape[1]
+    per = quarter // share
+    for p in range(pieces):
+        product = mm(grad_ref[p], mixed_ref[...], TN).astype(jnp.bfloat16)
+        for i in range(per):
+            part[p * per + i] = product[i * share : (i + 1) * share, :]
+    shares = []
+    for s in range(1, n):
+        peer = lax.rem(me + s, n)
+        shares.append(
+            pltpu.make_async_remote_copy(
+                src_ref=part.at[peer],
+                dst_ref=parts_in.at[s - 1],
+                send_sem=psend.at[s - 1],
+                recv_sem=precv.at[s - 1],
+                device_id={"sp": peer},
+                device_id_type=MESH,
+            )
+        )
+        shares[-1].start()
     change = []
     key_part = []
     for b in range(blocks):
@@ -212,6 +351,11 @@
             states_ref[b].astype(jnp.float32) * d_state, axis=0, keepdims=True
         )
         gg_ref[rows, :] = block_sums(triangle(False), gg_ref[rows, :] - moved) + at_end
+    summed = part[me].astype(jnp.float32)
+    for s in range(1, n):
+        shares[s - 1].wait()
+        summed = summed + parts_in[s - 1].astype(jnp.float32)
+    proj_ref[...] = summed
 
 
 def exchange_scratch(n, blocks, width, channels):
@@ -253,11 +397,12 @@
     )(q, k, v, g)
 
 
-def mixer_backward(q, k, v, g, d, states, scale):
+def mixer_backward(q, k, v, g, gathered, w_out, mixed, states, scale):
     n = lax.axis_size("sp")
     length, channels = q.shape
     width = v.shape[1]
     blocks = length // BLK
+    share = w_out.shape[0] // n
     return pl.pallas_call(
         functools.partial(backward_kernel, n, scale),
         out_shape=(
@@ -265,18 +410,81 @@
             jax.ShapeDtypeStruct((length, channels), jnp.bfloat16),
             jax.ShapeDtypeStruct((length, width), jnp.float32),
             jax.ShapeDtypeStruct((length, channels), jnp.float32),
-        ),
-        in_specs=in_vmem(6),
-        out_specs=tuple(in_vmem(4)),
-        scratch_shapes=exchange_scratch(n, blocks, width, channels),
+            jax.ShapeDtypeStruct((share, width), jnp.float32),
+        ),
+        in_specs=in_vmem(8),
+        out_specs=tuple(in_vmem(5)),
+        scratch_shapes=exchange_scratch(n, blocks, width, channels)
+        + [
+            pltpu.VMEM((length, width), jnp.bfloat16),
+            pltpu.VMEM((n, share, width), jnp.bfloat16),
+            pltpu.VMEM((n - 1, share, width), jnp.bfloat16),
+            pltpu.SemaphoreType.DMA((n - 1,)),
+            pltpu.SemaphoreType.DMA((n - 1,)),
+        ],
         compiler_params=pltpu.CompilerParams(
-            collective_id=2, has_side_effects=True, vmem_limit_bytes=16 * 1024 * 1024
+            collective_id=2, has_side_effects=True, vmem_limit_bytes=24 * 1024 * 1024
         ),
         cost_estimate=pl.CostEstimate(
             flops=8_000_000_000, bytes_accessed=4 * length * width, transcendentals=0
         ),
         name="mixer_backward",
-    )(q, k, v, g, d, states)
+    )(q, k, v, g, gathered, w_out, mixed, states)
+
+
+def route_out(d_out, route_expert, route_weight, capacity):
+    n, tp = lax.axis_size("sp"), lax.axis_size("tp")
+    tokens, model_width = d_out.shape
+    quarter = model_width // tp
+    return pl.pallas_call(
+        functools.partial(route_kernel, n, capacity),
+        out_shape=(
+            jax.ShapeDtypeStruct((n, capacity, quarter), jnp.bfloat16),
+            jax.ShapeDtypeStruct((2, tokens), jnp.int32),
+        ),
+        in_specs=in_vmem(3),
+        out_specs=tuple(in_vmem(2)),
+        scratch_shapes=[
+            pltpu.VMEM((n, capacity, quarter), jnp.bfloat16),
+            pltpu.SemaphoreType.DMA((n - 1,)),
+            pltpu.SemaphoreType.DMA((n - 1,)),
+            pltpu.SemaphoreType.DMA,
+        ],
+        compiler_params=pltpu.CompilerParams(
+            collective_id=3, has_side_effects=True, vmem_limit_bytes=24 * 1024 * 1024
+        ),
+        cost_estimate=pl.CostEstimate(
+            flops=8_000_000_000, bytes_accessed=4 * tokens * quarter, transcendentals=0
+        ),
+        name="route_out",
+    )(d_out, route_expert.T, route_weight)
+
+
+def route_back(summed, slots, d_out):
+    n, tp = lax.axis_size("sp"), lax.axis_size("tp")
+    capacity, quarter = summed.shape[1:]
+    tokens = d_out.shape[0]
+    return pl.pallas_call(
+        functools.partial(return_kernel, n, tp, capacity),
+        out_shape=jax.ShapeDtypeStruct((tp, tokens, quarter), jnp.bfloat16),
+        in_specs=in_vmem(3),
+        out_specs=in_vmem(1)[0],
+        scratch_shapes=[
+            pltpu.VMEM((n, capacity, quarter), jnp.bfloat16),
+            pltpu.SemaphoreType.DMA((n - 1,)),
+            pltpu.SemaphoreType.DMA((n - 1,)),
+            pltpu.SemaphoreType.DMA,
+            pltpu.SemaphoreType.DMA((tp,)),
+            pltpu.SemaphoreType.DMA((tp,)),
+        ],
+        compiler_params=pltpu.CompilerParams(
+            collective_id=4, has_side_effects=True, vmem_limit_bytes=24 * 1024 * 1024
+        ),
+        cost_estimate=pl.CostEstimate(
+            flops=8_000_000_000, bytes_accessed=4 * tokens * quarter, transcendentals=0
+        ),
+        name="route_back",
+    )(summed, slots, d_out)
 
 
 def expert_pass(rows_in, routed_rows, gate_w, up_w, down_w):
@@ -319,28 +527,11 @@
     values,
     log_decay,
 ):
-    tok_rows = d_out.shape[0]
     model_width = d_out.shape[1]
     experts = lax.axis_size("sp")
     capacity = expert_inputs.shape[1] // experts
-    flat_experts = route_expert.reshape(-1)
-    onehot = (flat_experts[:, None] == jnp.arange(experts, dtype=jnp.int32)[None, :]).astype(
-        jnp.int32
-    )
-    before = jnp.cumsum(onehot, axis=0) - onehot
-    rank_slot = jnp.sum(before * onehot, axis=1)
-    slot_index = flat_experts * capacity + rank_slot
     quarter = model_width // lax.axis_size("tp")
-    column_start = lax.axis_index("tp") * quarter
-    own_cols = lax.dynamic_slice_in_dim(d_out, column_start, quarter, 1)
-    scaled = (
-        jnp.repeat(own_cols, 2, axis=0).astype(jnp.float32) * route_weight.reshape(-1)[:, None]
-    ).astype(jnp.bfloat16)
-    outbox = (
-        jnp.zeros((experts * capacity, own_cols.shape[1]), jnp.bfloat16).at[slot_index].set(scaled)
-    )
-    outbox = outbox.reshape(experts, capacity, own_cols.shape[1])
-    partial_rows = lax.all_to_all(outbox, "sp", split_axis=0, concat_axis=0, tiled=True)
+    partial_rows, slots = route_out(d_out, route_expert, route_weight, capacity)
     routed = lax.all_gather(partial_rows, "tp", axis=2, tiled=True)
     routed = routed.reshape(experts * capacity, model_width)
     rows_in = expert_inputs[0]
@@ -357,26 +548,16 @@
     )
     rounded = lax.optimization_barrier(partial_terms.astype(jnp.bfloat16)).astype(jnp.float32)
     summed = lax.psum_scatter(rounded.astype(jnp.bfloat16), "tp", scatter_dimension=1, tiled=True)
-    returned = lax.all_to_all(
-        summed.reshape(experts, capacity, quarter), "sp", split_axis=0, concat_axis=0, tiled=True
-    )
-    picked = returned.reshape(experts * capacity, quarter)[slot_index].astype(jnp.float32)
-    picked = picked.reshape(tok_rows, 2, quarter).sum(axis=1)
-    mix_cols = (own_cols.astype(jnp.float32) + picked).astype(jnp.bfloat16)
-    mix_grad = lax.all_gather(mix_cols, "tp", axis=1, tiled=True)
     scale_q = queries.shape[2] ** (-0.5)
     q, k, v, g = queries[:, 0], keys[:, 0], values[:, 0], log_decay[:, 0]
     mixed, states = mixer_forward(q, k, v, g, scale_q)
-    grad_proj = lax.psum_scatter(
-        lax.dot_general(
-            mix_grad, mixed, (((0,), (0,)), ((), ())), preferred_element_type=jnp.float32
-        ).astype(jnp.bfloat16),
-        "sp",
-        scatter_dimension=0,
-        tiled=True,
-    ).astype(jnp.float32)
-    d_mixed = jnp.dot(mix_grad, w_out, preferred_element_type=jnp.float32).astype(jnp.bfloat16)
-    grad_q, grad_k, grad_v, grad_g = mixer_backward(q, k, v, g, d_mixed, states, scale_q)
+    summed, mixed, grad_gate, grad_up, grad_down = lax.optimization_barrier(
+        (summed, mixed, grad_gate, grad_up, grad_down)
+    )
+    gathered = route_back(summed.reshape(experts, capacity, quarter), slots, d_out)
+    grad_q, grad_k, grad_v, grad_g, grad_proj = mixer_backward(
+        q, k, v, g, gathered, w_out, mixed, states, scale_q
+    )
     return (
         grad_gate[None],
         grad_up[None],

time: 331 us -> 245 us (0.74)
  the two profiles are of different devices: /device:TPU:0 before, /device:TPU:12 now
where the time goes in v2:
time: 245 us
  Pallas kernels  131 us (53%)
  matrix products  54.9 us (22%)
  waiting for transfers between devices  30.4 us (12%)
  between operations  14.3 us (6%)
  local copies, waits for them, and re-layouts  13.4 us (5%)
    pallas_call x1, Pallas kernels, route_back(): pl.pallas_call(functools.partial(return_kernel, n, tp, capacity), out_sha...  45.2 us
    pallas_call x1, Pallas kernels, mixer_backward(): pl.pallas_call(functools.partial(backward_kernel, n, scale), out_shape=(j...  38.6 us
    pallas_call x1, Pallas kernels, route_out(): pl.pallas_call(functools.partial(route_kernel, n, capacity), out_shape=(j...  29.9 us
    all_gather x1, waiting for transfers between devices, local(): routed = lax.all_gather(partial_rows, 'tp', axis=2, tiled=True)  21.6 us
    pallas_call x1, Pallas kernels, mixer_forward(): pl.pallas_call(functools.partial(forward_kernel, n, scale), out_shape=(ja...  17.3 us
    unnamed x61, local copies, waits for them, and re-layouts  13.4 us
    dot_general x1, matrix products, expert_pass(): lax.dot_general(routed_rows, down_w, (((1,), (1,)), ((), ())), preferred_...  9.71 us
    reduce_scatter x1, waiting for transfers between devices, local(): lax.psum_scatter(rounded.astype(jnp.bfloat16), 'tp', scatter_dimension=1,...  8.83 us
  transfers between devices with their start and end apart: 2, of which 2 were waited for; matrix products, arithmetic and copies ran while one was open for 14% of the time, Pallas kernels for 7%

profile of v2, /device:TPU:12, one launch (start us, length us, event | category | flops | bytes accessed | tf_op | source)
XLA Modules:
  0.0 244.8 jit_solution(2446752150602365280)
XLA Ops:
  7.2 1.0 copy.20.weight_ref
  8.2 1.6 copy-done.2
  10.5 29.9 %route_out.1 = (bf16[8,144,512]{2,1,0:T(8,128)(2,1)S(1)}, s32[2,512]{1,0:T(2,128)S(1)}) custom-call(bf16[512,2048]{1,0:T(8,128)(2,1)S(1)} %copy-done.2, s32[2,512]{1,0:T(2,128)S(1)} %bitcast.71, f32[512,2]{1,0:T(8,128)S(1)} %copy.20.weight_ref), custom_call_target="tpu_custom_call" | custom-call | flops 8000000000 | bytes 1048576 | tf_op jit(solution)/shard_map/route_out/pallas_call | solution.py:439
  40.4 1.0 copy-done.1
  41.5 8.2 %fusion.4 = f32[1152,704]{0,1:T(8,128)} fusion(bf16[1,1152,2048]{2,1,0:T(8,128)(2,1)} %param.15, bf16[1,2048,704]{1,2,0:T(8,128)(2,1)S(1)} %copy-done), kind=kOutput, calls=%fused_computation.5 | convolution fusion | flops 3321888768 | bytes 10846208 | tf_op jit(solution)/shard_map/dot_general | solution.py:491
  49.7 8.6 %fusion.6 = f32[1152,704]{0,1:T(8,128)} fusion(bf16[1,1152,2048]{2,1,0:T(8,128)(2,1)} %param.15, bf16[1,2048,704]{1,2,0:T(8,128)(2,1)S(1)} %copy-done.16), kind=kOutput, calls=%fused_computation.7 | convolution fusion | flops 3321888768 | bytes 10846208 | tf_op jit(solution)/shard_map/dot_general | solution.py:492
  58.3 21.6 %all-gather.2.cloned.1.call-done = bf16[8,144,2048]{2,1,0:T(8,128)(2,1)} async-done(((bf16[8,144,512]{2,1,0:T(8,128)(2,1)}), bf16[8,144,2048]{2,1,0:T(8,128)(2,1)}) %all-gather.2.cloned.1.call-update) | async-done | bytes 4718608 | tf_op jit(solution)/shard_map/all_gather | solution.py:535
  79.9 9.7 %multiply_convert_fusion.1 = (bf16[1152,704]{0,1:T(8,128)(2,1)S(1)}, bf16[1152,704]{0,1:T(8,128)(2,1)S(1)}) fusion(f32[1152,704]{0,1:T(8,128)} %fusion.4, f32[1152,704]{0,1:T(8,128)} %fusion.6, bf16[1152,2048]{1,0:T(8,128)(2,1)} %bitcast.74, bf16[1,704,2048]{2,1,0:T(8,128)(2,1)} %param.18), kind=kOutput, calls=%fused_computation.13 | convolution fusion | flops 3332431872 | bytes 17334272 | tf_op jit(solution)/shard_map/dot_general | solution.py:496
  89.6 4.1 %fusion.21 = f32[1152,2048]{1,0:T(8,128)S(1)} fusion(bf16[1152,704]{0,1:T(8,128)(2,1)S(1)} %get-tuple-element.45, bf16[1,2048,704]{1,2,0:T(8,128)(2,1)S(1)} %copy-done), kind=kOutput, calls=%fused_computation.19 | convolution fusion | flops 3321888768 | bytes 13942784 | tf_op jit(solution)/shard_map/dot_general | solution.py:543
  93.8 5.9 %add_convert_fusion = bf16[1152,2048]{1,0:T(8,128)(2,1)} fusion(f32[1152,2048]{1,0:T(8,128)S(1)} %fusion.21, bf16[1152,704]{0,1:T(8,128)(2,1)S(1)} %get-tuple-element.44, bf16[1,2048,704]{1,2,0:T(8,128)(2,1)S(1)} %copy-done.17), kind=kOutput, calls=%fused_computation | convolution fusion | flops 3326607360 | bytes 18661376 | tf_op jit(solution)/shard_map/dot_general | solution.py:546
  99.7 0.9 copy-done.6
  100.8 0.9 copy-done.9
  101.7 17.3 %mixer_forward.1 = (bf16[512,256]{1,0:T(8,128)(2,1)S(1)}, bf16[8,256,128]{2,1,0:T(8,128)(2,1)S(1)}) custom-call(bf16[512,128]{1,0:T(8,128)(2,1)S(1)} %bitcast.67, bf16[512,128]{1,0:T(8,128)(2,1)S(1)} %bitcast.69, bf16[512,256]{1,0:T(8,128)(2,1)S(1)} %bitcast.63, f32[512,128]{1,0:T(8,128)S(1)} %bitcast.65), custom_call_target="tpu_custom_call" | custom-call | flops 4000000000 | bytes 524288 | tf_op jit(solution)/shard_map/mixer_forward/pallas_call | solution.py:381
  119.0 0.8 copy-done.12
  120.5 7.8 %fusion.15 = bf16[2048,704]{0,1:T(8,128)(2,1)} fusion(bf16[1152,704]{0,1:T(8,128)(2,1)S(1)} %copy-done.23, bf16[1,1152,2048]{2,1,0:T(8,128)(2,1)} %param.15), kind=kOutput, calls=%fused_computation.17 | convolution fusion | flops 3323330560 | bytes 9224192 | tf_op jit(solution)/shard_map/dot_general | solution.py:507
  128.3 5.2 %fusion.18 = bf16[2048,704]{0,1:T(8,128)(2,1)} fusion(bf16[1152,704]{0,1:T(8,128)(2,1)S(1)} %copy-done.19, bf16[1,1152,2048]{2,1,0:T(8,128)(2,1)S(1)} %bitcast.73), kind=kOutput, calls=%fused_computation.18 | convolution fusion | flops 3323330560 | bytes 9224192 | tf_op jit(solution)/shard_map/dot_general | solution.py:504
  133.5 5.4 %convolution_convert_fusion = bf16[704,2048]{1,0:T(8,128)(2,1)} fusion(bf16[1152,2048]{1,0:T(8,128)(2,1)S(1)} %bitcast.77, f32[1152,704]{0,1:T(8,128)S(1)} %copy-done.21, f32[1152,704]{0,1:T(8,128)S(1)} %copy-done.20), kind=kOutput, calls=%fused_computation.11 | convolution fusion | flops 3328196608 | bytes 14090240 | tf_op jit(solution)/shard_map/dot_general | solution.py:510
  138.9 8.8 %reduce-scatter.2.cloned.1.call-done = bf16[1152,512]{1,0:T(8,128)(2,1)} async-done(((bf16[1152,2048]{1,0:T(8,128)(2,1)}), bf16[1152,512]{1,0:T(8,128)(2,1)}) %reduce-scatter.2.cloned.1.call-update) | async-done | bytes 1179664 | tf_op jit(solution)/shard_map/reduce_scatter | solution.py:550
  147.7 1.6 copy-done.3
  149.3 1.3 copy-done.4
  150.6 45.2 %route_back.1.grad_ref = bf16[4,512,512]{2,1,0:T(8,128)(2,1)S(1)} custom-call(bf16[8,144,512]{2,1,0:T(8,128)(2,1)S(1)} %bitcast.62, s32[2,512]{1,0:T(2,128)S(1)} %get-tuple-element.28.slot_ref, bf16[512,2048]{1,0:T(8,128)(2,1)S(1)} %copy-done.3), custom_call_target="tpu_custom_call" | custom-call | flops 8000000000 | bytes 1048576 | tf_op jit(solution)/shard_map/route_back/pallas_call | solution.py:467
  195.9 38.6 %mixer_backward.1 = (bf16[512,128]{1,0:T(8,128)(2,1)S(1)}, bf16[512,128]{1,0:T(8,128)(2,1)S(1)}, f32[512,256]{1,0:T(8,128)S(1)}, f32[512,128]{1,0:T(8,128)S(1)}, f32[256,256]{1,0:T(8,128)S(1)}) custom-call(bf16[512,128]{1,0:T(8,128)(2,1)S(1)} %bitcast.68, bf16[512,128]{1,0:T(8,128)(2,1)S(1)} %bitcast.70, bf16[512,256]{1,0:T(8,128)(2,1)S(1)} %bitcast.64, ...), custom_call_target="tpu_custom_call" | custom-call | flops 8000000000 | bytes 524288 | tf_op jit(solution)/shard_map/mixer_backward/pallas_call | solution.py:406
  234.5 0.7 convert_bitcast_fusion
  235.2 0.7 copy.26
  (58 shorter events, 3.7 us)
Async XLA Ops:
  7.2 34.3 %copy-start = (bf16[1,2048,704]{1,2,0:T(8,128)(2,1)S(1)}, bf16[1,2048,704]{1,2,0:T(8,128)(2,1)}, u32[]{:S(2)}) copy-start(bf16[1,2048,704]{1,2,0:T(8,128)(2,1)} %param.16) | copy-start | bytes 8650756
  7.2 72.7 %all-gather.2.cloned.1.call-start = ((), (), s32[]{:S(2)}) async-start(), calls=%async_computation.1 | async-start | bytes 5898240 | tf_op jit(solution)/shard_map/all_gather | solution.py:535
  8.2 1.6 copy-start.2
  41.5 106.3 %reduce-scatter.2.cloned.1.call-start = ((), (), s32[]{:S(2)}) async-start(), calls=%async_computation.2 | async-start | bytes 5898240 | tf_op jit(solution)/shard_map/reduce_scatter | solution.py:550
  41.5 8.2 %copy-start.16 = (bf16[1,2048,704]{1,2,0:T(8,128)(2,1)S(1)}, bf16[1,2048,704]{1,2,0:T(8,128)(2,1)}, u32[]{:S(2)}) copy-start(bf16[1,2048,704]{1,2,0:T(8,128)(2,1)} %param.17) | copy-start | bytes 8650756
  89.6 4.2 %copy-start.18 = (bf16[1152,704]{0,1:T(8,128)(2,1)}, bf16[1152,704]{0,1:T(8,128)(2,1)S(1)}, u32[]{:S(2)}) copy-start(bf16[1152,704]{0,1:T(8,128)(2,1)S(1)} %get-tuple-element.45) | copy-start | bytes 4866052
  89.6 4.2 %copy-start.22 = (bf16[1152,704]{0,1:T(8,128)(2,1)}, bf16[1152,704]{0,1:T(8,128)(2,1)S(1)}, u32[]{:S(2)}) copy-start(bf16[1152,704]{0,1:T(8,128)(2,1)S(1)} %get-tuple-element.44) | copy-start | bytes 4866052
  89.6 4.2 %copy-start.17 = (bf16[1,2048,704]{1,2,0:T(8,128)(2,1)S(1)}, bf16[1,2048,704]{1,2,0:T(8,128)(2,1)}, u32[]{:S(2)}) copy-start(bf16[1,2048,704]{1,2,0:T(8,128)(2,1)} %param.17) | copy-start | bytes 8650756
  99.7 1.0 copy-start.7
  99.7 1.1 copy-start.8
  101.7 18.8 %copy-start.23 = (bf16[1152,704]{0,1:T(8,128)(2,1)S(1)}, bf16[1152,704]{0,1:T(8,128)(2,1)}, u32[]{:S(2)}) copy-start(bf16[1152,704]{0,1:T(8,128)(2,1)} %copy-done.22) | copy-start | bytes 4866052
  101.7 26.6 %slice-start = ((s8[4718592]{0:T(1024)(128)(4,1)}), s8[4194304]{0:T(1024)(128)(4,1)S(1)}, s32[]{:S(2)}) async-start(s8[4718592]{0:T(1024)(128)(4,1)} %bitcast.72), calls=%async_computation.3 | async-start | bytes 8388608
  120.5 7.8 %slice-start.1 = ((s8[4718592]{0:T(1024)(128)(4,1)}), s8[524288]{0:T(1024)(128)(4,1)S(1)}, s32[]{:S(2)}) async-start(s8[4718592]{0:T(1024)(128)(4,1)} %bitcast.72), calls=%async_computation.4 | async-start | bytes 1048576
  120.5 7.8 %copy-start.19 = (bf16[1152,704]{0,1:T(8,128)(2,1)S(1)}, bf16[1152,704]{0,1:T(8,128)(2,1)}, u32[]{:S(2)}) copy-start(bf16[1152,704]{0,1:T(8,128)(2,1)} %copy-done.18) | copy-start | bytes 4866052
  120.5 13.0 %slice-start.2 = ((s8[4718592]{0:T(1024)(128)(4,1)}), s8[4194304]{0:T(1024)(128)(4,1)S(1)}, s32[]{:S(2)}) async-start(s8[4718592]{0:T(1024)(128)(4,1)} %bitcast.75), calls=%async_computation.5 | async-start | bytes 8388608
  128.3 5.2 %slice-start.3 = ((s8[4718592]{0:T(1024)(128)(4,1)}), s8[524288]{0:T(1024)(128)(4,1)S(1)}, s32[]{:S(2)}) async-start(s8[4718592]{0:T(1024)(128)(4,1)} %bitcast.75), calls=%async_computation.6 | async-start | bytes 1048576
  128.3 5.2 %copy-start.20 = (f32[1152,704]{0,1:T(8,128)S(1)}, f32[1152,704]{0,1:T(8,128)}, u32[]{:S(2)}) copy-start(f32[1152,704]{0,1:T(8,128)} %fusion.4) | copy-start | bytes 9732100
  128.3 5.2 %copy-start.21 = (f32[1152,704]{0,1:T(8,128)S(1)}, f32[1152,704]{0,1:T(8,128)}, u32[]{:S(2)}) copy-start(f32[1152,704]{0,1:T(8,128)} %fusion.6) | copy-start | bytes 9732100
  147.7 1.6 copy-start.3
  149.3 1.3 copy-start.4
  150.6 45.2 %copy-start.5 = (bf16[2048,256]{1,0:T(8,128)(2,1)S(1)}, bf16[2048,256]{1,0:T(8,128)(2,1)}, u32[]{:S(2)}) copy-start(bf16[2048,256]{1,0:T(8,128)(2,1)} %w_ref.1) | copy-start | bytes 3145732
  150.6 45.2 %copy-start.10 = (bf16[512,1,128]{2,0,1:T(8,128)(2,1)S(1)}, bf16[512,1,128]{2,0,1:T(8,128)(2,1)}, u32[]{:S(2)}) copy-start(bf16[512,1,128]{2,0,1:T(8,128)(2,1)} %param.21) | copy-start | bytes 393220
  150.6 45.3 %copy-start.13 = (bf16[8,256,128]{2,1,0:T(8,128)(2,1)S(1)}, bf16[8,256,128]{2,1,0:T(8,128)(2,1)}, u32[]{:S(2)}) copy-start(bf16[8,256,128]{2,1,0:T(8,128)(2,1)} %copy-done.12) | copy-start | bytes 1572868
  150.6 45.3 %copy-start.15 = (bf16[512,256]{1,0:T(8,128)(2,1)S(1)}, bf16[512,256]{1,0:T(8,128)(2,1)}, u32[]{:S(2)}) copy-start(bf16[512,256]{1,0:T(8,128)(2,1)} %copy-done.14) | copy-start | bytes 786436
  (6 other events, 5.1 us)
Sparse Core Ops, SparseCore 0:
  41.6 38.2 all-gather.1
  99.9 47.8 reduce-scatter.1

commit v3 on v2

--- a/solution.py
+++ b/solution.py
@@ -52,9 +52,27 @@
     return barrier, len(others)
 
 
-def route_kernel(n, cap, d_ref, expert_ref, weight_ref, arrived_ref, slot_ref, outbox, ssem, rsem, lsem):
+def route_kernel(
+    n,
+    tp,
+    cap,
+    d_ref,
+    expert_ref,
+    weight_ref,
+    routed_ref,
+    slot_ref,
+    outbox,
+    ssem,
+    rsem,
+    lsem,
+    tsend,
+    trecv,
+):
     me = lax.axis_index("sp")
-    barrier, greeted = greet(n, me)
+    col = lax.axis_index("tp")
+    partner = col + 1 - 2 * lax.rem(col, 2)
+    far = [lax.rem(col + 2 * s, tp) for s in range(1, tp // 2)]
+    barrier, greeted = greet(n, me, [partner] + far)
     tokens = d_ref.shape[0]
     quarter = outbox.shape[2]
     start = pl.multiple_of(lax.axis_index("tp") * quarter, quarter)
@@ -80,7 +98,68 @@
             rows = rows + mm(picks, scaled[j], NN)
         outbox[e] = rows.astype(jnp.bfloat16)
     pl.semaphore_wait(barrier, greeted)
-    exchange(n, me, outbox, arrived_ref, ssem, rsem, lsem)
+
+    def place(row, column):
+        return routed_ref.at[row, :, pl.ds(pl.multiple_of(column * quarter, quarter), quarter)]
+
+    copies = []
+    for k in range(1, n):
+        peer = lax.rem(me + k, n)
+        copies.append(
+            pltpu.make_async_remote_copy(
+                src_ref=outbox.at[peer],
+                dst_ref=place(me, col),
+                send_sem=ssem.at[k - 1],
+                recv_sem=rsem.at[k - 1],
+                device_id={"sp": peer},
+                device_id_type=MESH,
+            )
+        )
+        copies[-1].start()
+    stays = pltpu.make_async_copy(outbox.at[me], place(me, col), lsem)
+    stays.start()
+
+    def send(k, column, slot, target):
+        row = lax.rem(me - k + n, n)
+        return pltpu.make_async_remote_copy(
+            src_ref=place(row, column),
+            dst_ref=place(row, column),
+            send_sem=tsend.at[k, slot],
+            recv_sem=trecv.at[k, slot],
+            device_id={"tp": target},
+            device_id_type=MESH,
+        )
+
+    across, beside, passed = [], [], []
+
+    def pass_on(k):
+        for s in range(len(far)):
+            across[k][s].wait_recv()
+            column = lax.rem(col - 2 * (s + 1) + tp, tp)
+            passed.append(send(k, column, tp // 2 + s, partner))
+            passed[-1].start()
+
+    for k in range(n):
+        if k == 0:
+            stays.wait()
+        else:
+            copies[k - 1].wait_recv()
+        across.append([send(k, col, s + 1, far[s]) for s in range(len(far))])
+        for copy in across[k]:
+            copy.start()
+        beside.append(send(k, col, 0, partner))
+        beside[k].start()
+        if k > 1:
+            pass_on(k - 2)
+    for k in range(max(n - 2, 0), n):
+        pass_on(k)
+    for copy in copies:
+        copy.wait_send()
+    for row in across:
+        for copy in row:
+            copy.wait_send()
+    for copy in beside + passed:
+        copy.wait()
 
 
 def exchange(n, me, source, target, ssem, rsem, lsem):
@@ -255,6 +334,8 @@
     rsem,
     d_ref,
     part,
+    pair_in,
+    pair,
     parts_in,
     psend,
     precv,
@@ -287,26 +368,24 @@
     copies = state_copies(n, me, -1, send, recv, ssem, rsem)
     for copy in copies:
         copy.start()
-    share = part.shape[1]
+    half, share = part.shape[1:3]
     per = quarter // share
     for p in range(pieces):
         product = mm(grad_ref[p], mixed_ref[...], TN).astype(jnp.bfloat16)
         for i in range(per):
-            part[p * per + i] = product[i * share : (i + 1) * share, :]
-    shares = []
-    for s in range(1, n):
-        peer = lax.rem(me + s, n)
-        shares.append(
-            pltpu.make_async_remote_copy(
-                src_ref=part.at[peer],
-                dst_ref=parts_in.at[s - 1],
-                send_sem=psend.at[s - 1],
-                recv_sem=precv.at[s - 1],
-                device_id={"sp": peer},
-                device_id_type=MESH,
-            )
-        )
-        shares[-1].start()
+            at = p * per + i
+            part[at % 2, at // 2] = product[i * share : (i + 1) * share, :]
+    parity = lax.rem(me, 2)
+    mine = me // 2
+    pairing = pltpu.make_async_remote_copy(
+        src_ref=part.at[1 - parity],
+        dst_ref=pair_in,
+        send_sem=psend.at[0],
+        recv_sem=precv.at[0],
+        device_id={"sp": me + 1 - 2 * parity},
+        device_id_type=MESH,
+    )
+    pairing.start()
     change = []
     key_part = []
     for b in range(blocks):
@@ -334,7 +413,26 @@
         key_part.append(d_lifted_k * fall)
         gg_ref[rows, :] = change[b]
         gv_ref[rows, :] = mm(scores, d_out, TN).astype(gv_ref.dtype)
+    pairing.wait()
+    for i in range(half):
+        pair[i] = (part[parity, i].astype(jnp.float32) + pair_in[i].astype(jnp.float32)).astype(
+            jnp.bfloat16
+        )
     collect(n, me, -1, copies, recv, total, width)
+    shares = []
+    for s in range(1, half):
+        other = lax.rem(mine + s, half)
+        shares.append(
+            pltpu.make_async_remote_copy(
+                src_ref=pair.at[other],
+                dst_ref=parts_in.at[s - 1],
+                send_sem=psend.at[s],
+                recv_sem=precv.at[s],
+                device_id={"sp": 2 * other + parity},
+                device_id_type=MESH,
+            )
+        )
+        shares[-1].start()
     for b in range(blocks):
         rows = pl.ds(b * BLK, BLK)
         cumulative, _, ending = decays(g_ref, rows)
@@ -351,8 +449,8 @@
             states_ref[b].astype(jnp.float32) * d_state, axis=0, keepdims=True
         )
         gg_ref[rows, :] = block_sums(triangle(False), gg_ref[rows, :] - moved) + at_end
-    summed = part[me].astype(jnp.float32)
-    for s in range(1, n):
+    summed = pair[mine].astype(jnp.float32)
+    for s in range(1, half):
         shares[s - 1].wait()
         summed = summed + parts_in[s - 1].astype(jnp.float32)
     proj_ref[...] = summed
@@ -417,10 +515,12 @@
         scratch_shapes=exchange_scratch(n, blocks, width, channels)
         + [
             pltpu.VMEM((length, width), jnp.bfloat16),
-            pltpu.VMEM((n, share, width), jnp.bfloat16),
-            pltpu.VMEM((n - 1, share, width), jnp.bfloat16),
-            pltpu.SemaphoreType.DMA((n - 1,)),
-            pltpu.SemaphoreType.DMA((n - 1,)),
+            pltpu.VMEM((2, n // 2, share, width), jnp.bfloat16),
+            pltpu.VMEM((n // 2, share, width), jnp.bfloat16),
+            pltpu.VMEM((n // 2, share, width), jnp.bfloat16),
+            pltpu.VMEM((n // 2 - 1, share, width), jnp.bfloat16),
+            pltpu.SemaphoreType.DMA((n // 2,)),
+            pltpu.SemaphoreType.DMA((n // 2,)),
         ],
         compiler_params=pltpu.CompilerParams(
             collective_id=2, has_side_effects=True, vmem_limit_bytes=24 * 1024 * 1024
@@ -437,9 +537,9 @@
     tokens, model_width = d_out.shape
     quarter = model_width // tp
     return pl.pallas_call(
-        functools.partial(route_kernel, n, capacity),
+        functools.partial(route_kernel, n, tp, capacity),
         out_shape=(
-            jax.ShapeDtypeStruct((n, capacity, quarter), jnp.bfloat16),
+            jax.ShapeDtypeStruct((n, capacity, model_width), jnp.bfloat16),
             jax.ShapeDtypeStruct((2, tokens), jnp.int32),
         ),
         in_specs=in_vmem(3),
@@ -449,6 +549,8 @@
             pltpu.SemaphoreType.DMA((n - 1,)),
             pltpu.SemaphoreType.DMA((n - 1,)),
             pltpu.SemaphoreType.DMA,
+            pltpu.SemaphoreType.DMA((n, tp)),
+            pltpu.SemaphoreType.DMA((n, tp)),
         ],
         compiler_params=pltpu.CompilerParams(
             collective_id=3, has_side_effects=True, vmem_limit_bytes=24 * 1024 * 1024
@@ -531,8 +633,7 @@
     experts = lax.axis_size("sp")
     capacity = expert_inputs.shape[1] // experts
     quarter = model_width // lax.axis_size("tp")
-    partial_rows, slots = route_out(d_out, route_expert, route_weight, capacity)
-    routed = lax.all_gather(partial_rows, "tp", axis=2, tiled=True)
+    routed, slots = route_out(d_out, route_expert, route_weight, capacity)
     routed = routed.reshape(experts * capacity, model_width)
     rows_in = expert_inputs[0]
     gate_w = w_gate[0]

time: 245 us -> 221 us (0.902)
  the two profiles are of different devices: /device:TPU:12 before, /device:TPU:0 now
where the time goes in v3:
time: 221 us; the launch traced here: 220 us
  Pallas kernels  140 us (63%)
  matrix products  43.8 us (20%)
  between operations  14.4 us (7%)
  local copies, waits for them, and re-layouts  10.9 us (5%)
  waiting for transfers between devices  10.2 us (5%)
    pallas_call x1, Pallas kernels, route_out(): pl.pallas_call(functools.partial(route_kernel, n, tp, capacity), out_shap...  42.4 us
    pallas_call x1, Pallas kernels, mixer_backward(): pl.pallas_call(functools.partial(backward_kernel, n, scale), out_shape=(j...  40.6 us
    pallas_call x1, Pallas kernels, route_back(): pl.pallas_call(functools.partial(return_kernel, n, tp, capacity), out_sha...  37.6 us
    pallas_call x1, Pallas kernels, mixer_forward(): pl.pallas_call(functools.partial(forward_kernel, n, scale), out_shape=(ja...  19.1 us
    unnamed x67, local copies, waits for them, and re-layouts  10.9 us
    reduce_scatter x1, waiting for transfers between devices, local(): lax.psum_scatter(rounded.astype(jnp.bfloat16), 'tp', scatter_dimension=1,...  10.2 us
    dot_general x1, matrix products, expert_pass(): lax.dot_general(rows_in, d_up, rows_first, preferred_element_type=jnp.flo...  8.37 us
    dot_general x1, matrix products, expert_pass(): gate_pre = jnp.dot(rows_in, gate_w, preferred_element_type=jnp.float32)  6.41 us
  transfers between devices with their start and end apart: 1, of which 1 were waited for; matrix products, arithmetic and copies ran while one was open for 9% of the time, Pallas kernels for 9%

profile of v3, /device:TPU:0, one launch (start us, length us, event | category | flops | bytes accessed | tf_op | source)
XLA Modules:
  0.0 219.8 jit_solution(9402427892228701306)
XLA Ops:
  7.2 1.0 copy.20.weight_ref
  8.2 0.8 copy-done
  9.0 6.4 %fusion.4 = f32[1152,704]{0,1:T(8,128)S(1)} fusion(bf16[1,1152,2048]{2,1,0:T(8,128)(2,1)} %param.15, bf16[1,2048,704]{1,2,0:T(8,128)(2,1)S(1)} %copy-done), kind=kOutput, calls=%fused_computation.5 | convolution fusion | flops 3321888768 | bytes 10846208 | tf_op jit(solution)/shard_map/dot_general | solution.py:593
  15.5 4.0 %fusion.6 = f32[1152,704]{0,1:T(8,128)S(1)} fusion(bf16[1,1152,2048]{2,1,0:T(8,128)(2,1)S(1)} %copy-done.16, bf16[1,2048,704]{1,2,0:T(8,128)(2,1)S(1)} %copy-done.18), kind=kOutput, calls=%fused_computation.7 | convolution fusion | flops 3321888768 | bytes 10846208 | tf_op jit(solution)/shard_map/dot_general | solution.py:594
  19.5 42.4 %route_out.1 = (bf16[8,144,2048]{2,1,0:T(8,128)(2,1)S(1)}, s32[2,512]{1,0:T(2,128)S(1)}) custom-call(bf16[512,2048]{1,0:T(8,128)(2,1)S(1)} %copy-done.1, s32[2,512]{1,0:T(2,128)S(1)} %bitcast.71, f32[512,2]{1,0:T(8,128)S(1)} %copy.20.weight_ref), custom_call_target="tpu_custom_call" | custom-call | flops 8000000000 | bytes 1048576 | tf_op jit(solution)/shard_map/route_out/pallas_call | solution.py:539
  62.0 4.8 %multiply_convert_fusion.1 = (bf16[1152,704]{0,1:T(8,128)(2,1)S(1)}, bf16[1152,704]{0,1:T(8,128)(2,1)S(1)}) fusion(f32[1152,704]{0,1:T(8,128)S(1)} %fusion.4, f32[1152,704]{0,1:T(8,128)S(1)} %fusion.6, bf16[1152,2048]{1,0:T(8,128)(2,1)S(1)} %bitcast.72, bf16[1,704,2048]{2,1,0:T(8,128)(2,1)S(1)} %copy-done.17), kind=kOutput, calls=%fused_computation.13 | convolution fusion | flops 3332431872 | bytes 17334272 | tf_op jit(solution)/shard_map/dot_general | solution.py:598
  66.8 3.9 %fusion.21 = f32[1152,2048]{1,0:T(8,128)S(1)} fusion(bf16[1152,704]{0,1:T(8,128)(2,1)S(1)} %get-tuple-element.45, bf16[1,2048,704]{1,2,0:T(8,128)(2,1)S(1)} %copy-done), kind=kOutput, calls=%fused_computation.19 | convolution fusion | flops 3321888768 | bytes 13942784 | tf_op jit(solution)/shard_map/dot_general | solution.py:644
  70.8 5.7 %add_convert_fusion = bf16[1152,2048]{1,0:T(8,128)(2,1)} fusion(f32[1152,2048]{1,0:T(8,128)S(1)} %fusion.21, bf16[1152,704]{0,1:T(8,128)(2,1)S(1)} %get-tuple-element.44, bf16[1,2048,704]{1,2,0:T(8,128)(2,1)S(1)} %copy-done.18), kind=kOutput, calls=%fused_computation | convolution fusion | flops 3326607360 | bytes 18661376 | tf_op jit(solution)/shard_map/dot_general | solution.py:647
  76.5 0.9 copy-done.5
  77.6 0.9 copy-done.8
  78.5 19.1 %mixer_forward.1 = (bf16[512,256]{1,0:T(8,128)(2,1)S(1)}, bf16[8,256,128]{2,1,0:T(8,128)(2,1)S(1)}) custom-call(bf16[512,128]{1,0:T(8,128)(2,1)S(1)} %bitcast.67, bf16[512,128]{1,0:T(8,128)(2,1)S(1)} %bitcast.69, bf16[512,256]{1,0:T(8,128)(2,1)S(1)} %bitcast.63, f32[512,128]{1,0:T(8,128)S(1)} %bitcast.65), custom_call_target="tpu_custom_call" | custom-call | flops 4000000000 | bytes 524288 | tf_op jit(solution)/shard_map/mixer_forward/pallas_call | solution.py:479
  97.6 0.8 copy-done.12
  98.4 0.7 copy-done.14
  99.1 8.4 %fusion.15 = bf16[2048,704]{0,1:T(8,128)(2,1)} fusion(bf16[1152,704]{0,1:T(8,128)(2,1)S(1)} %copy-done.26, bf16[1,1152,2048]{2,1,0:T(8,128)(2,1)} %param.15), kind=kOutput, calls=%fused_computation.17 | convolution fusion | flops 3323330560 | bytes 9224192 | tf_op jit(solution)/shard_map/dot_general | solution.py:609
  107.6 5.2 %fusion.18 = bf16[2048,704]{0,1:T(8,128)(2,1)} fusion(bf16[1152,704]{0,1:T(8,128)(2,1)S(1)} %copy-done.20, bf16[1,1152,2048]{2,1,0:T(8,128)(2,1)S(1)} %bitcast.77), kind=kOutput, calls=%fused_computation.18 | convolution fusion | flops 3323330560 | bytes 9224192 | tf_op jit(solution)/shard_map/dot_general | solution.py:606
  112.8 5.4 %convolution_convert_fusion = bf16[704,2048]{1,0:T(8,128)(2,1)} fusion(bf16[1152,2048]{1,0:T(8,128)(2,1)S(1)} %bitcast.75, f32[1152,704]{0,1:T(8,128)S(1)} %copy-done.24, f32[1152,704]{0,1:T(8,128)S(1)} %copy-done.22), kind=kOutput, calls=%fused_computation.11 | convolution fusion | flops 3328196608 | bytes 14090240 | tf_op jit(solution)/shard_map/dot_general | solution.py:612
  118.1 10.2 %reduce-scatter.2.cloned.1.call-done = bf16[1152,512]{1,0:T(8,128)(2,1)} async-done(((bf16[1152,2048]{1,0:T(8,128)(2,1)}), bf16[1152,512]{1,0:T(8,128)(2,1)}) %reduce-scatter.2.cloned.1.call-update) | async-done | bytes 1179664 | tf_op jit(solution)/shard_map/reduce_scatter | solution.py:651
  128.3 1.6 copy-done.2
  129.9 1.3 copy-done.3
  131.2 37.6 %route_back.1.grad_ref = bf16[4,512,512]{2,1,0:T(8,128)(2,1)S(1)} custom-call(bf16[8,144,512]{2,1,0:T(8,128)(2,1)S(1)} %bitcast.62, s32[2,512]{1,0:T(2,128)S(1)} %get-tuple-element.28.slot_ref, bf16[512,2048]{1,0:T(8,128)(2,1)S(1)} %copy-done.2), custom_call_target="tpu_custom_call" | custom-call | flops 8000000000 | bytes 1048576 | tf_op jit(solution)/shard_map/route_back/pallas_call | solution.py:569
  168.9 40.6 %mixer_backward.1 = (bf16[512,128]{1,0:T(8,128)(2,1)S(1)}, bf16[512,128]{1,0:T(8,128)(2,1)S(1)}, f32[512,256]{1,0:T(8,128)S(1)}, f32[512,128]{1,0:T(8,128)S(1)}, f32[256,256]{1,0:T(8,128)S(1)}) custom-call(bf16[512,128]{1,0:T(8,128)(2,1)S(1)} %bitcast.68, bf16[512,128]{1,0:T(8,128)(2,1)S(1)} %bitcast.70, bf16[512,256]{1,0:T(8,128)(2,1)S(1)} %bitcast.64, ...), custom_call_target="tpu_custom_call" | custom-call | flops 8000000000 | bytes 524288 | tf_op jit(solution)/shard_map/mixer_backward/pallas_call | solution.py:504
  209.5 0.7 convert_bitcast_fusion
  210.2 0.7 copy.26
  212.3 0.7 copy.29
  (61 shorter events, 1.6 us)
Async XLA Ops:
  7.2 1.8 copy-start
  7.2 121.1 %reduce-scatter.2.cloned.1.call-start = ((), (), s32[]{:S(2)}) async-start(), calls=%async_computation.1 | async-start | bytes 5898240 | tf_op jit(solution)/shard_map/reduce_scatter | solution.py:651
  9.0 6.4 %copy-start.16 = (bf16[1,1152,2048]{2,1,0:T(8,128)(2,1)S(1)}, bf16[1,1152,2048]{2,1,0:T(8,128)(2,1)}, u32[]{:S(2)}) copy-start(bf16[1,1152,2048]{2,1,0:T(8,128)(2,1)} %param.15) | copy-start | bytes 14155780
  9.0 6.4 %copy-start.18 = (bf16[1,2048,704]{1,2,0:T(8,128)(2,1)S(1)}, bf16[1,2048,704]{1,2,0:T(8,128)(2,1)}, u32[]{:S(2)}) copy-start(bf16[1,2048,704]{1,2,0:T(8,128)(2,1)} %param.17) | copy-start | bytes 8650756
  15.4 46.5 %copy-start.21 = (f32[1152,704]{0,1:T(8,128)}, f32[1152,704]{0,1:T(8,128)S(1)}, u32[]{:S(2)}) copy-start(f32[1152,704]{0,1:T(8,128)S(1)} %fusion.4) | copy-start | bytes 9732100
  15.5 4.1 %copy-start.1 = (bf16[512,2048]{1,0:T(8,128)(2,1)S(1)}, bf16[512,2048]{1,0:T(8,128)(2,1)}, u32[]{:S(2)}) copy-start(bf16[512,2048]{1,0:T(8,128)(2,1)} %d_ref.3) | copy-start | bytes 6291460
  15.5 4.1 %copy-start.10 = (s32[512,2]{0,1:T(2,128)S(1)}, s32[512,2]{0,1:T(2,128)}, u32[]{:S(2)}) copy-start(s32[512,2]{0,1:T(2,128)} %param.13) | copy-start | bytes 12292
  19.5 42.5 %copy-start.23 = (f32[1152,704]{0,1:T(8,128)}, f32[1152,704]{0,1:T(8,128)S(1)}, u32[]{:S(2)}) copy-start(f32[1152,704]{0,1:T(8,128)S(1)} %fusion.6) | copy-start | bytes 9732100
  19.5 42.4 %copy-start.17 = (bf16[1,704,2048]{2,1,0:T(8,128)(2,1)S(1)}, bf16[1,704,2048]{2,1,0:T(8,128)(2,1)}, u32[]{:S(2)}) copy-start(bf16[1,704,2048]{2,1,0:T(8,128)(2,1)} %param.18) | copy-start | bytes 8650756
  61.9 4.8 %copy-start.11 = (bf16[8,144,2048]{2,1,0:T(8,128)(2,1)}, bf16[8,144,2048]{2,1,0:T(8,128)(2,1)S(1)}, u32[]{:S(2)}) copy-start(bf16[8,144,2048]{2,1,0:T(8,128)(2,1)S(1)} %get-tuple-element.22) | copy-start | bytes 14155780
  66.8 4.0 %copy-start.19 = (bf16[1152,704]{0,1:T(8,128)(2,1)}, bf16[1152,704]{0,1:T(8,128)(2,1)S(1)}, u32[]{:S(2)}) copy-start(bf16[1152,704]{0,1:T(8,128)(2,1)S(1)} %get-tuple-element.45) | copy-start | bytes 4866052
  66.8 4.0 %copy-start.25 = (bf16[1152,704]{0,1:T(8,128)(2,1)}, bf16[1152,704]{0,1:T(8,128)(2,1)S(1)}, u32[]{:S(2)}) copy-start(bf16[1152,704]{0,1:T(8,128)(2,1)S(1)} %get-tuple-element.44) | copy-start | bytes 4866052
  78.5 20.7 %copy-start.26 = (bf16[1152,704]{0,1:T(8,128)(2,1)S(1)}, bf16[1152,704]{0,1:T(8,128)(2,1)}, u32[]{:S(2)}) copy-start(bf16[1152,704]{0,1:T(8,128)(2,1)} %copy-done.25) | copy-start | bytes 4866052
  78.5 29.0 %slice-start.2 = ((s8[4718592]{0:T(1024)(128)(4,1)}), s8[4194304]{0:T(1024)(128)(4,1)S(1)}, s32[]{:S(2)}) async-start(s8[4718592]{0:T(1024)(128)(4,1)} %bitcast.76), calls=%async_computation.4 | async-start | bytes 8388608
  99.1 8.4 %slice-start.3 = ((s8[4718592]{0:T(1024)(128)(4,1)}), s8[524288]{0:T(1024)(128)(4,1)S(1)}, s32[]{:S(2)}) async-start(s8[4718592]{0:T(1024)(128)(4,1)} %bitcast.76), calls=%async_computation.5 | async-start | bytes 1048576
  99.1 8.4 %copy-start.20 = (bf16[1152,704]{0,1:T(8,128)(2,1)S(1)}, bf16[1152,704]{0,1:T(8,128)(2,1)}, u32[]{:S(2)}) copy-start(bf16[1152,704]{0,1:T(8,128)(2,1)} %copy-done.19) | copy-start | bytes 4866052
  99.1 13.6 %slice-start = ((s8[4718592]{0:T(1024)(128)(4,1)}), s8[4194304]{0:T(1024)(128)(4,1)S(1)}, s32[]{:S(2)}) async-start(s8[4718592]{0:T(1024)(128)(4,1)} %bitcast.73), calls=%async_computation.2 | async-start | bytes 8388608
  107.5 5.2 %slice-start.1 = ((s8[4718592]{0:T(1024)(128)(4,1)}), s8[524288]{0:T(1024)(128)(4,1)S(1)}, s32[]{:S(2)}) async-start(s8[4718592]{0:T(1024)(128)(4,1)} %bitcast.73), calls=%async_computation.3 | async-start | bytes 1048576
  107.5 5.2 %copy-start.22 = (f32[1152,704]{0,1:T(8,128)S(1)}, f32[1152,704]{0,1:T(8,128)}, u32[]{:S(2)}) copy-start(f32[1152,704]{0,1:T(8,128)} %copy-done.21) | copy-start | bytes 9732100
  107.5 5.2 %copy-start.24 = (f32[1152,704]{0,1:T(8,128)S(1)}, f32[1152,704]{0,1:T(8,128)}, u32[]{:S(2)}) copy-start(f32[1152,704]{0,1:T(8,128)} %copy-done.23) | copy-start | bytes 9732100
  131.2 37.6 %copy-start.4 = (bf16[2048,256]{1,0:T(8,128)(2,1)S(1)}, bf16[2048,256]{1,0:T(8,128)(2,1)}, u32[]{:S(2)}) copy-start(bf16[2048,256]{1,0:T(8,128)(2,1)} %w_ref.1) | copy-start | bytes 3145732
  131.2 37.7 %copy-start.9 = (bf16[512,1,128]{2,0,1:T(8,128)(2,1)S(1)}, bf16[512,1,128]{2,0,1:T(8,128)(2,1)}, u32[]{:S(2)}) copy-start(bf16[512,1,128]{2,0,1:T(8,128)(2,1)} %param.21) | copy-start | bytes 393220
  131.2 37.7 %copy-start.13 = (bf16[8,256,128]{2,1,0:T(8,128)(2,1)S(1)}, bf16[8,256,128]{2,1,0:T(8,128)(2,1)}, u32[]{:S(2)}) copy-start(bf16[8,256,128]{2,1,0:T(8,128)(2,1)} %copy-done.12) | copy-start | bytes 1572868
  131.2 37.7 %copy-start.15 = (bf16[512,256]{1,0:T(8,128)(2,1)S(1)}, bf16[512,256]{1,0:T(8,128)(2,1)}, u32[]{:S(2)}) copy-start(bf16[512,256]{1,0:T(8,128)(2,1)} %copy-done.14) | copy-start | bytes 786436
  (8 other events, 8.3 us)
Sparse Core Ops, SparseCore 0:
  76.6 51.6 reduce-scatter.1
